TPU v7x, 32 devices: a whole 2x2x4 slice. The times are simulated.
32 devices in a mesh: sp: 8 (over z, y), dp: 4 (over x, core).
Axes of the slice: x: 2, y: 2, z: 4, core: 2. Of those that a mesh axis runs over, the one named last changes fastest.
Arguments:
- tokens: bfloat16 [4, 2048, 2048], P('dp', 'sp'), may hold values from -6 to 6
- w_query: bfloat16 [2048, 2048], P('dp', 'sp'), may hold values from -0.125 to 0.125
- w_key: bfloat16 [2048, 1024], P('dp', 'sp'), may hold values from -0.125 to 0.125
- w_value: bfloat16 [2048, 1024], P('dp', 'sp'), may hold values from -0.125 to 0.125
- w_out: bfloat16 [2048, 2048], P('dp', 'sp'), may hold values from -0.25 to 0.25
- qk_gain: float32 [2, 128], replicated, may hold values from 0.9 to 24
Outputs:
- mixed_out: bfloat16 [4, 2048, 2048], P('dp', 'sp')
All inputs are finite; a program needn't handle non-finite values.
Results may differ from a plain program's by a relative error of at most 0.006.
The roundings to bfloat16 on the way count: a program that leaves them out, or rounds other values in their place, can miss the bound.
Values may be sent and summed in bfloat16 or wider, within the bound.
No kernel may reach another device: no remote copies, remote signals or barrier semaphores. Data moves between devices by JAX's collectives and lax.ppermute only.
A program may use at most 64 MiB of HBM per device.

v0:
```python
import math

import jax
import jax.numpy as jnp
import numpy as np
from jax import lax
from jax.sharding import PartitionSpec as P

HQ = 16
KV = 8
HD = 128
GRID_W = 64


ROPE_BASE = 10000.0
EPS = 1e-06


def angles(positions):
    quarter = jnp.arange(0, HD // 2, 2, dtype=jnp.float32)
    inv_freq = ROPE_BASE ** (-quarter / (HD // 2))
    row_pos = (positions // GRID_W).astype(jnp.float32)
    col_pos = (positions % GRID_W).astype(jnp.float32)
    angle_table = jnp.concatenate(
        [row_pos[:, None] * inv_freq, col_pos[:, None] * inv_freq], axis=1
    )
    return (jnp.cos(angle_table), jnp.sin(angle_table))


def prepare(raw_proj, gain_row, cosine, sine_table):
    normed = (
        raw_proj * lax.rsqrt(jnp.mean(raw_proj * raw_proj, axis=-1, keepdims=True) + EPS) * gain_row
    )
    pair_view = normed.reshape(raw_proj.shape[:-1] + (HD // 2, 2))
    first_half = pair_view[..., 0]
    second = pair_view[..., 1]
    cos_b = cosine[:, None, :]
    sin_b = sine_table[:, None, :]
    turned = jnp.stack(
        [first_half * cos_b - second * sin_b, first_half * sin_b + second * cos_b], axis=-1
    )
    return turned.reshape(raw_proj.shape).astype(jnp.bfloat16)


def attend_head(query_rows, key_rows, value_rows):
    seq_len = query_rows.shape[0]
    block_len = math.gcd(seq_len, 512)
    blocks = query_rows.reshape(seq_len // block_len, block_len, HD)

    def one_block(row_block):
        scores = jnp.dot(row_block, key_rows.T, preferred_element_type=jnp.float32) * HD ** (-0.5)
        top_score = jnp.max(scores, axis=1, keepdims=True)
        weights = jnp.exp(scores - top_score)
        row_total = jnp.sum(weights, axis=1, keepdims=True)
        probs_bf = (weights / row_total).astype(jnp.bfloat16)
        return jnp.dot(probs_bf, value_rows, preferred_element_type=jnp.float32).astype(
            jnp.bfloat16
        )

    return lax.map(one_block, blocks).reshape(seq_len, HD)


def project(own_rows, weight):
    col_full = lax.all_gather(weight, "sp", axis=1, tiled=True)
    return jnp.dot(
        own_rows,
        lax.all_gather(col_full, "dp", axis=0, tiled=True),
        preferred_element_type=jnp.float32,
    )


def on_device(tokens, w_query, w_key, w_value, w_out, qk_gain):
    own_rows = tokens[0]
    n_seqdev = lax.axis_size("sp")
    tok_local = own_rows.shape[0]
    positions = lax.axis_index("sp") * tok_local + jnp.arange(tok_local, dtype=jnp.int32)
    cosine, sine_table = angles(positions)
    heads_dev = HQ // n_seqdev
    group_size = HQ // KV
    kv_dev = max(1, heads_dev // group_size)
    chosen = (np.arange(n_seqdev) * heads_dev // group_size)[:, None] + np.arange(kv_dev)[None, :]
    chosen = chosen.reshape(-1)
    key_all = prepare(
        project(own_rows, w_key).reshape(tok_local, KV, HD), qk_gain[1], cosine, sine_table
    )
    values = project(own_rows, w_value).astype(jnp.bfloat16).reshape(tok_local, KV, HD)
    key_send = key_all[:, chosen, :].reshape(tok_local, -1)
    value_send = values[:, chosen, :].reshape(tok_local, -1)
    raw_proj = project(own_rows, w_query).reshape(tok_local, HQ, HD)
    query_heads = lax.all_to_all(
        prepare(raw_proj, qk_gain[0], cosine, sine_table).reshape(tok_local, HQ * HD),
        "sp",
        split_axis=1,
        concat_axis=0,
        tiled=True,
    )
    key_heads = lax.all_to_all(key_send, "sp", split_axis=1, concat_axis=0, tiled=True)
    value_heads = lax.all_to_all(value_send, "sp", split_axis=1, concat_axis=0, tiled=True)
    outputs = []
    for head_index in range(heads_dev):
        kv_slot = head_index // group_size if heads_dev >= group_size else 0
        outputs.append(
            attend_head(
                query_heads[:, head_index * HD : (head_index + 1) * HD],
                key_heads[:, kv_slot * HD : (kv_slot + 1) * HD],
                value_heads[:, kv_slot * HD : (kv_slot + 1) * HD],
            )
        )
    mixed_heads = jnp.concatenate(outputs, axis=1)
    token_rows = lax.all_to_all(mixed_heads, "sp", split_axis=0, concat_axis=1, tiled=True)
    return project(token_rows, w_out).astype(jnp.bfloat16)[None]


def solution(mesh):
    in_specs = (
        P("dp", "sp", None),
        P("dp", "sp"),
        P("dp", "sp"),
        P("dp", "sp"),
        P("dp", "sp"),
        P(),
    )
    out_specs = P("dp", "sp", None)
    return jax.shard_map(
        on_device, mesh=mesh, in_specs=in_specs, out_specs=out_specs, check_vma=False
    )
```

profile of v0, /device:TPU:0, one launch (start us, length us, event | category | flops | bytes accessed | tf_op | source)
XLA Modules:
  0.0 416.6 jit_solution(12027826076929534750)
XLA Ops:
  8.8 42.7 %all-gather.17.cloned.1.call-done = bf16[512,1024]{1,0:T(8,128)(2,1)} async-done(((bf16[512,128]{1,0:T(8,128)(2,1)}), bf16[512,1024]{1,0:T(8,128)(2,1)}) %all-gather.17.cloned.1.call-update) | async-done | bytes 1048592 | tf_op jit(solution)/shard_map/all_gather | solution.py:64
  51.6 51.4 %all-gather.9.cloned.1.call-done = bf16[512,2048]{1,0:T(8,128)(2,1)} async-done(((bf16[512,256]{1,0:T(8,128)(2,1)}), bf16[512,2048]{1,0:T(8,128)(2,1)}) %all-gather.9.cloned.1.call-update) | async-done | bytes 2097168 | tf_op jit(solution)/shard_map/all_gather | solution.py:64
  103.0 39.6 %all-gather.13.cloned.1.call-done = bf16[512,1024]{1,0:T(8,128)(2,1)} async-done(((bf16[512,128]{1,0:T(8,128)(2,1)}), bf16[512,1024]{1,0:T(8,128)(2,1)}) %all-gather.13.cloned.1.call-update) | async-done | bytes 1048592 | tf_op jit(solution)/shard_map/all_gather | solution.py:64
  143.8 33.7 %all-gather.19.cloned.1.call-done = bf16[2048,1024]{1,0:T(8,128)(2,1)} async-done(((bf16[512,1024]{1,0:T(8,128)(2,1)}), bf16[2048,1024]{1,0:T(8,128)(2,1)}) %all-gather.19.cloned.1.call-update) | async-done | bytes 4194320 | tf_op jit(solution)/shard_map/all_gather | solution.py:67
  177.6 3.4 fusion.21
  182.6 5.5 %all-to-all-start.2 = ((bf16[256,8,128]{2,0,1:T(8,128)(2,1)}), bf16[256,8,128]{2,0,1:T(8,128)(2,1)}, u32[]{:S(2)}, u32[]{:S(2)}) async-start(bf16[256,8,128]{2,0,1:T(8,128)(2,1)} %bitcast.19), calls=%async_computation.2 | async-start | bytes 1048576 | tf_op jit(solution)/shard_map/all_to_all | solution.py:98
  188.1 49.2 %all-gather.11.cloned.1.call-done = bf16[2048,2048]{1,0:T(8,128)(2,1)} async-done(((bf16[512,2048]{1,0:T(8,128)(2,1)}), bf16[2048,2048]{1,0:T(8,128)(2,1)}) %all-gather.11.cloned.1.call-update) | async-done | bytes 8388624 | tf_op jit(solution)/shard_map/all_gather | solution.py:67
  237.3 12.2 %copy.19 = bf16[2048,2048]{1,0:T(8,128)(2,1)} copy(bf16[2048,2048]{0,1:T(8,128)(2,1)} %bitcast.93) | data formatting | bytes 16777216 | tf_op jit(solution)/shard_map/dot_general | solution.py:65
  249.5 5.8 %multiply_reduce_fusion.2 = (f32[256,16]{0,1:T(8,128)S(1)}, f32[256,16,128]{0,2,1:T(8,128)S(1)}) fusion(bf16[16,128,2048]{2,1,0:T(8,128)(2,1)} %bitcast.94, bf16[1,256,2048]{2,1,0:T(8,128)(2,1)S(1)} %copy-done), kind=kOutput, calls=%fused_computation.31 | convolution fusion | flops 2148528128 | bytes 11550720 | tf_op jit(solution)/shard_map/dot_general | solution.py:65
  257.0 2.5 reshape.165
  259.5 2.9 subtract_convert_fusion
  262.4 2.4 pad_maximum_fusion
  266.1 5.5 %all-to-all-start = ((bf16[256,8,256]{0,2,1:T(8,128)(2,1)}), bf16[256,8,256]{0,2,1:T(8,128)(2,1)S(1)}, u32[]{:S(2)}, u32[]{:S(2)}) async-start(bf16[256,8,256]{0,2,1:T(8,128)(2,1)} %convert_element_type.44), calls=%async_computation | async-start | bytes 2097152 | tf_op jit(solution)/shard_map/all_to_all | solution.py:90
  273.2 6.5 %copy.21 = bf16[1024,2048]{1,0:T(8,128)(2,1)} copy(bf16[1024,2048]{0,1:T(8,128)(2,1)} %bitcast.96) | data formatting | bytes 8388608 | tf_op jit(solution)/shard_map/dot_general | solution.py:65
  279.7 3.5 multiply_reduce_fusion.3
  286.1 20.1 %all-to-all-done = bf16[256,8,256]{0,2,1:T(8,128)(2,1)S(1)} async-done(((bf16[256,8,256]{0,2,1:T(8,128)(2,1)}), bf16[256,8,256]{0,2,1:T(8,128)(2,1)S(1)}, u32[]{:S(2)}, u32[]{:S(2)}) %all-to-all-start) | async-done | bytes 1048608 | tf_op jit(solution)/shard_map/all_to_all | solution.py:90
  306.2 3.5 all-to-all-start.1
  309.8 31.3 %all-gather.21.cloned.1.call-done = bf16[512,2048]{1,0:T(8,128)(2,1)} async-done(((bf16[512,256]{1,0:T(8,128)(2,1)}), bf16[512,2048]{1,0:T(8,128)(2,1)}) %all-gather.21.cloned.1.call-update) | async-done | bytes 2097168 | tf_op jit(solution)/shard_map/all_gather | solution.py:64
  341.8 15.1 %while.21 = (s32[]{:T(128)}, bf16[4,512,128]{2,1,0:T(8,128)(2,1)S(1)}, bf16[4,512,128]{2,1,0:T(8,128)(2,1)S(1)}, bf16[2048,128]{1,0:T(8,128)(2,1)S(1)}, bf16[2048,128]{1,0:T(8,128)(2,1)}, /*index=5*/s32[]{:T(128)}) while((s32[]{:T(128)}, bf16[4,512,128]{2,1,0:T(8,128)(2,1)S(1)}, bf16[4,512,128]{2,1,0:T(8,128)(2,1)S(1)}, ...), condition=%wide.region_9.10_spmd, body=%wide.region_6.9_spmd.sunk | while | flops 546372608 | bytes 13903957 | solution.py:60
  347.2 2.2 fusion.57
  350.9 2.2 fusion.57
  357.0 14.9 %while.20 = (s32[]{:T(128)}, bf16[4,512,128]{2,1,0:T(8,128)(2,1)S(1)}, bf16[4,512,128]{2,1,0:T(8,128)(2,1)S(1)}, bf16[2048,128]{1,0:T(8,128)(2,1)S(1)}, bf16[2048,128]{1,0:T(8,128)(2,1)}, /*index=5*/s32[]{:T(128)}) while((s32[]{:T(128)}, bf16[4,512,128]{2,1,0:T(8,128)(2,1)S(1)}, bf16[4,512,128]{2,1,0:T(8,128)(2,1)S(1)}, ...), condition=%wide.region_5.6_spmd, body=%wide.region_2.5_spmd.sunk | while | flops 546372608 | bytes 13903957 | solution.py:60
  372.0 30.4 %all_to_all.64 = bf16[8,256,256]{2,1,0:T(8,128)(2,1)S(1)} all-to-all(bf16[8,256,256]{2,1,0:T(8,128)(2,1)S(1)} %pad_maximum_fusion.1), channel_id=1, replica_groups=mesh['sp'=8,'dp'=4] {'sp'}, dimensions={0} | all-to-all | bytes 2097152 | tf_op jit(solution)/shard_map/all_to_all | solution.py:110
  403.0 6.8 %fusion.20 = bf16[1,256,2048]{2,1,0:T(8,128)(2,1)} fusion(bf16[256,2048]{0,1:T(8,128)(2,1)S(1)} %bitcast.95, bf16[2048,2048]{1,0:T(8,128)(2,1)} %all-gather.23.cloned.1.call-done), kind=kOutput, calls=%fused_computation.29 | convolution fusion | flops 2148007936 | bytes 10485760 | tf_op jit(solution)/shard_map/dot_general | solution.py:65
  (73 shorter events, 39.3 us)
Async XLA Ops:
  6.5 171.0 %copy-start = (bf16[1,256,2048]{2,1,0:T(8,128)(2,1)S(1)}, bf16[1,256,2048]{2,1,0:T(8,128)(2,1)}, u32[]{:S(2)}) copy-start(bf16[1,256,2048]{2,1,0:T(8,128)(2,1)} %param.13) | copy-start | bytes 3145732
  6.5 136.9 %copy-start.2 = (f32[2,128]{1,0:T(2,128)S(1)}, f32[2,128]{1,0:T(2,128)}, u32[]{:S(2)}) copy-start(f32[2,128]{1,0:T(2,128)} %param.18) | copy-start | bytes 3076
  6.5 45.0 %all-gather.17.cloned.1.call-start = ((), (), s32[]{:S(2)}) async-start(), calls=%async_computation.8 | async-start | bytes 1179648 | tf_op jit(solution)/shard_map/all_gather | solution.py:64
  7.3 95.7 %all-gather.9.cloned.1.call-start = ((), (), s32[]{:S(2)}) async-start(), calls=%async_computation.4 | async-start | bytes 2359296 | tf_op jit(solution)/shard_map/all_gather | solution.py:64
  8.0 134.6 %all-gather.13.cloned.1.call-start = ((), (), s32[]{:S(2)}) async-start(), calls=%async_computation.6 | async-start | bytes 1179648 | tf_op jit(solution)/shard_map/all_gather | solution.py:64
  8.7 168.8 %all-gather.19.cloned.1.call-start = ((), (), s32[]{:S(2)}) async-start(), calls=%async_computation.9 | async-start | bytes 5242880 | tf_op jit(solution)/shard_map/all_gather | solution.py:67
  51.6 185.7 %all-gather.11.cloned.1.call-start = ((), (), s32[]{:S(2)}) async-start(), calls=%async_computation.5 | async-start | bytes 10485760 | tf_op jit(solution)/shard_map/all_gather | solution.py:67
  103.0 170.2 %all-gather.15.cloned.1.call-start = ((), (), s32[]{:S(2)}) async-start(), calls=%async_computation.7 | async-start | bytes 5242880 | tf_op jit(solution)/shard_map/all_gather | solution.py:67
  142.7 198.4 %all-gather.21.cloned.1.call-start = ((), (), s32[]{:S(2)}) async-start(), calls=%async_computation.10 | async-start | bytes 2359296 | tf_op jit(solution)/shard_map/all_gather | solution.py:64
  182.6 83.5 %all-to-all-start.2 = ((bf16[256,8,128]{2,0,1:T(8,128)(2,1)}), bf16[256,8,128]{2,0,1:T(8,128)(2,1)}, u32[]{:S(2)}, u32[]{:S(2)}) async-start(bf16[256,8,128]{2,0,1:T(8,128)(2,1)} %bitcast.19), calls=%async_computation.2 | async-start | bytes 1048576 | tf_op jit(solution)/shard_map/all_to_all | solution.py:98
  266.1 40.1 %all-to-all-start = ((bf16[256,8,256]{0,2,1:T(8,128)(2,1)}), bf16[256,8,256]{0,2,1:T(8,128)(2,1)S(1)}, u32[]{:S(2)}, u32[]{:S(2)}) async-start(bf16[256,8,256]{0,2,1:T(8,128)(2,1)} %convert_element_type.44), calls=%async_computation | async-start | bytes 2097152 | tf_op jit(solution)/shard_map/all_to_all | solution.py:90
  306.2 35.5 %all-to-all-start.1 = ((bf16[256,8,128]{2,0,1:T(8,128)(2,1)}), bf16[256,8,128]{2,0,1:T(8,128)(2,1)S(1)}, u32[]{:S(2)}, u32[]{:S(2)}) async-start(bf16[256,8,128]{2,0,1:T(8,128)(2,1)} %bitcast.16), calls=%async_computation.1 | async-start | bytes 1048576 | tf_op jit(solution)/shard_map/all_to_all | solution.py:97
  309.7 93.2 %all-gather.23.cloned.1.call-start = ((), (), s32[]{:S(2)}) async-start(), calls=%async_computation.11 | async-start | bytes 10485760 | tf_op jit(solution)/shard_map/all_gather | solution.py:67
  403.0 6.8 %copy-start.1 = (bf16[1,256,2048]{2,1,0:T(8,128)(2,1)S(1)}, bf16[1,256,2048]{2,1,0:T(8,128)(2,1)}, u32[]{:S(2)}) copy-start(bf16[1,256,2048]{2,1,0:T(8,128)(2,1)} %param.13) | copy-start | bytes 3145732
Sparse Core Ops, SparseCore 0:
  9.4 42.1 all-gather.16
  53.6 49.3 all-gather.8
  105.0 37.5 all-gather.12
  144.0 33.4 all-gather.18
  179.0 58.2 all-gather.10
  238.7 34.4 all-gather.14
  275.2 65.8 all-gather.20
  342.6 57.7 all-gather.22
where the time goes:
time: 418 us; the launch traced here: 417 us
  waiting for transfers between devices  273 us (65%)
  matrix products  42.8 us (10%)
  blocking collectives  30.4 us (7%)
  local copies, waits for them, and re-layouts  27.8 us (7%)
  starting transfers between devices  14.8 us (4%)
  other arithmetic  14.5 us (3%)
  between operations  13.7 us (3%)
    all_gather x4, waiting for transfers between devices, project(): col_full = lax.all_gather(weight, 'sp', axis=1, tiled=True)  165 us
    all_gather x4, waiting for transfers between devices, project(): lax.all_gather(col_full, 'dp', axis=0, tiled=True)  84.5 us
    all_to_all x1, blocking collectives, on_device(): lax.all_to_all(mixed_heads, 'sp', split_axis=0, concat_axis=1, tiled=True)  30.4 us
    all_to_all x1, waiting for transfers between devices, on_device(): lax.all_to_all(prepare(raw_proj, qk_gain[0], cosine, sine_table).reshape(...  20.1 us
    dot_general x4, matrix products, project(): jnp.dot(own_rows, lax.all_gather(col_full, 'dp', axis=0, tiled=True), pre...  19.5 us
    dot_general x2, local copies, waits for them, and re-layouts, project(): jnp.dot(own_rows, lax.all_gather(col_full, 'dp', axis=0, tiled=True), pre...  18.7 us
    dot_general x8, matrix products, one_block(): jnp.dot(probs_bf, value_rows, preferred_element_type=jnp.float32)  17 us
  transfers between devices with their start and end apart: 11, of which 8 were waited for; matrix products, arithmetic and copies ran while one was open for 19% of the time, Pallas kernels for 0%

commit v1 on v0

v1 whole, which is shorter than its diff:
```python
import functools
import math

import jax
import jax.numpy as jnp
from jax import lax
from jax.experimental import pallas as pl
from jax.experimental.pallas import tpu as pltpu
from jax.sharding import PartitionSpec as P


HQ = 16
KV = 8
HD = 128
GRID_W = 64

ROPE_BASE = 10000.0
EPS = 1e-06
LOG2E = 1.4426950408889634


def rotary_tables(seq_len):
    positions = jnp.arange(seq_len, dtype=jnp.int32)
    quarter = jnp.arange(0, HD // 2, 2, dtype=jnp.float32)
    inv_freq = jnp.repeat(ROPE_BASE ** (-quarter / (HD // 2)), 2)
    row_pos = (positions // GRID_W).astype(jnp.float32)
    col_pos = (positions % GRID_W).astype(jnp.float32)
    angle = jnp.concatenate([row_pos[:, None] * inv_freq, col_pos[:, None] * inv_freq], axis=1)
    sign = jnp.where(jnp.arange(HD) % 2 == 0, -1.0, 1.0).astype(jnp.float32)
    return jnp.cos(angle), jnp.sin(angle) * sign


def shift(n_outer, n_inner, outer):
    pairs = []
    for a in range(n_outer):
        for b in range(n_inner):
            to = ((a + 1) % n_outer, b) if outer else (a, (b + 1) % n_inner)
            pairs.append((a * n_inner + b, to[0] * n_inner + to[1]))
    return pairs


def send_back(n_outer, n_inner, i, j):
    return [
        (a * n_inner + b, (a - i) % n_outer * n_inner + (b - j) % n_inner)
        for a in range(n_outer)
        for b in range(n_inner)
    ]


def owner_of(axis, n_outer, n_inner, i, j):
    me = lax.axis_index(axis)
    return lax.rem(me // n_inner + 2 * n_outer - i, n_outer) * n_inner + lax.rem(
        lax.rem(me, n_inner) + 2 * n_inner - j, n_inner
    )


def whole(shape):
    return pl.BlockSpec(shape, lambda i, ix: (0,) * len(shape))


ANY = pl.BlockSpec(memory_space=pl.ANY)


def params(mib):
    return pltpu.CompilerParams(vmem_limit_bytes=mib * 2**20)


def assemble_kernel(places, index_ref, *refs):
    block_refs, (out_ref, sem) = refs[:-2], refs[-2:]
    copies = []
    for t, (b, lead, row, col) in enumerate(places):
        src = block_refs[b] if lead is None else block_refs[b].at[lead]
        height, width = src.shape
        to = out_ref
        if row is not None:
            to = to.at[pl.ds(pl.multiple_of(index_ref[row] * height, height), height)]
        if col is not None:
            to = to.at[:, pl.ds(pl.multiple_of(index_ref[col] * width, width), width)]
        copies.append(pltpu.make_async_copy(src, to, sem.at[t]))
        copies[-1].start()
    for copy in copies:
        copy.wait()


def assemble(blocks, places, index, shape):
    return pl.pallas_call(
        functools.partial(assemble_kernel, places),
        out_shape=jax.ShapeDtypeStruct(shape, jnp.bfloat16),
        grid_spec=pltpu.PrefetchScalarGridSpec(
            num_scalar_prefetch=1,
            grid=(1,),
            in_specs=[ANY] * len(blocks),
            out_specs=whole(shape),
            scratch_shapes=[pltpu.SemaphoreType.DMA((len(places),))],
        ),
        cost_estimate=pl.CostEstimate(
            flops=1000 * math.prod(shape), bytes_accessed=4 * math.prod(shape), transcendentals=0
        ),
        compiler_params=params(8),
        name="assemble",
    )(index, *blocks)


def project_kernel(n_b, n_x, n_q, n_kv, first, index_ref, *refs):
    x_refs, refs = refs[:n_x], refs[n_x:]
    cos_refs, refs = refs[:n_b], refs[n_b:]
    sin_refs, refs = refs[:n_b], refs[n_b:]
    gain_ref, w_ref = refs[:2]
    outs, held, x_whole, x_sem, sem = refs[-9:-6], refs[-6:-3], refs[-3], refs[-2], refs[-1]
    q_ref, k_ref, v_ref = held
    loads = []
    for t in range(n_x):
        height = x_refs[t].shape[0]
        loads.append(pltpu.make_async_copy(x_refs[t], x_whole.at[pl.ds(t * height, height)], x_sem.at[t]))
        loads[-1].start()
    q_width, kv_width = n_q * HD, n_kv * HD
    even = lax.broadcasted_iota(jnp.int32, cos_refs[0].shape, 1) % 2 == 0
    rows = q_ref.shape[1]
    copies = []
    for b in range(n_b):
        for load in loads[b * n_x // n_b : (b + 1) * n_x // n_b]:
            load.wait()
        x = x_whole[b * rows : (b + 1) * rows, :]
        total = jnp.dot(x, w_ref[...], preferred_element_type=jnp.float32)
        cos, sin = cos_refs[b][...], sin_refs[b][...]

        def turned(raw, gain):
            normed = raw * lax.rsqrt(jnp.mean(raw * raw, axis=-1, keepdims=True) + EPS) * gain
            other = jnp.where(even, pltpu.roll(normed, HD - 1, 1), pltpu.roll(normed, 1, 1))
            return (normed * cos + other * sin).astype(jnp.bfloat16)

        for h in range(n_q):
            at = h * HD
            q_ref[b, :, at : at + HD] = turned(total[:, at : at + HD], gain_ref[0:1, :])
        for h in range(n_kv):
            at = h * HD
            raw = total[:, q_width + at : q_width + at + HD]
            k_ref[b, :, at : at + HD] = turned(raw, gain_ref[1:2, :])
        v_ref[b] = total[:, q_width + kv_width :].astype(jnp.bfloat16)
    for i in range(3):
        copies.append(pltpu.make_async_copy(held[i], outs[i].at[pl.ds(first, n_b)], sem.at[i]))
        copies[-1].start()
    for copy in copies:
        copy.wait()


def project(blocks, slots, first, weight, index, n_d, gain, cos, sin, n_q, n_kv, held, n_all):
    halves = [half for block in blocks for half in block]
    n_b, n_x = len(blocks), len(halves)
    depth = halves[0].shape[1]
    rows = halves[0].shape[0] * n_x // n_b
    width = weight.shape[1]
    at_rows = [pl.BlockSpec((rows, HD), lambda i, ix, s=s: (ix[n_d + s], 0)) for s in slots]
    in_specs = [ANY] * n_x + at_rows + at_rows + [whole(gain.shape), whole(weight.shape)]
    args = [*halves, *[cos] * n_b, *[sin] * n_b, gain, weight]
    aliases = {}
    if held is not None:
        aliases = {1 + len(args) + i: i for i in range(3)}
        in_specs += [ANY] * 3
        args += list(held)
    widths = (n_q * HD, n_kv * HD, n_kv * HD)
    return pl.pallas_call(
        functools.partial(project_kernel, n_b, n_x, n_q, n_kv, first),
        out_shape=[jax.ShapeDtypeStruct((n_all, rows, w), jnp.bfloat16) for w in widths],
        grid_spec=pltpu.PrefetchScalarGridSpec(
            num_scalar_prefetch=1,
            grid=(1,),
            in_specs=in_specs,
            out_specs=[ANY] * 3,
            scratch_shapes=[pltpu.VMEM((n_b, rows, w), jnp.bfloat16) for w in widths]
            + [
                pltpu.VMEM((n_b * rows, depth), jnp.bfloat16),
                pltpu.SemaphoreType.DMA((n_x,)),
                pltpu.SemaphoreType.DMA((3,)),
            ],
        ),
        input_output_aliases=aliases,
        cost_estimate=pl.CostEstimate(
            flops=4 * n_b * rows * depth * width,
            bytes_accessed=2 * (n_b * rows * depth + depth * width + n_b * rows * width),
            transcendentals=0,
        ),
        compiler_params=params(20),
        name="project",
    )(index, *args)


def attend_kernel(n_q, group, qs, keys, carried, final, q_ref, k_ref, v_ref, *refs):
    if carried:
        acc_in, ml_in = refs[:2]
    outs = refs[-(qs[1] - qs[0]) :] if final else refs[-2:]
    rows = q_ref.shape[1]
    scale = HD**-0.5 * LOG2E

    def one(b, out_ref):
        for h in range(n_q):
            at = (h // group) * HD
            cols = slice(h * HD, (h + 1) * HD)
            some = k_ref[keys[0] : keys[1], :, at : at + HD].reshape((keys[1] - keys[0]) * rows, HD)
            values = v_ref[keys[0] : keys[1], :, at : at + HD].reshape((keys[1] - keys[0]) * rows, HD)
            scores = lax.dot_general(
                q_ref[b, :, cols], some, (((1,), (1,)), ((), ())), preferred_element_type=jnp.float32
            )
            top = jnp.max(scores, axis=1, keepdims=True)
            if carried:
                top_in = ml_in[b, :, 2 * h : 2 * h + 1]
                top = jnp.maximum(top, top_in)
                fade = jnp.exp2((top_in - top) * scale)
            weights = jnp.exp2((scores - top) * scale)
            total = jnp.sum(weights, axis=1, keepdims=True)
            out = jnp.dot(weights.astype(jnp.bfloat16), values, preferred_element_type=jnp.float32)
            if carried:
                total = total + fade * ml_in[b, :, 2 * h + 1 : 2 * h + 2]
                out = out + fade * acc_in[b, :, cols]
            if final:
                out_ref[:, cols] = (out * (1.0 / total)).astype(jnp.bfloat16)
            else:
                outs[0][b, :, cols] = out
                outs[1][b, :, 2 * h : 2 * h + 1] = top
                outs[1][b, :, 2 * h + 1 : 2 * h + 2] = total

    if final:
        for b in range(*qs):
            one(b, outs[b - qs[0]])
    else:
        pl.loop(*qs)(lambda b: one(b, None))


def attend(held, state, qs, keys, carried, final, n_q, group):
    query, key, value = held
    n_all, rows, _ = query.shape
    n_kv = key.shape[2] // HD
    vmem = pl.BlockSpec(memory_space=pltpu.VMEM)
    args, in_specs, aliases = [query, key, value], [vmem] * 3, {}
    if state is not None and (carried or not final):
        in_specs += [vmem if carried else ANY] * 2
        args += list(state)
    if final:
        out_shape = [jax.ShapeDtypeStruct((rows, n_q * HD), jnp.bfloat16)] * (qs[1] - qs[0])
    else:
        out_shape = [
            jax.ShapeDtypeStruct((n_all, rows, n_q * HD), jnp.float32),
            jax.ShapeDtypeStruct((n_all, rows, 128), jnp.float32),
        ]
        if state is not None:
            aliases = {3: 0, 4: 1}
    n_pairs = (qs[1] - qs[0]) * (keys[1] - keys[0])
    return pl.pallas_call(
        functools.partial(attend_kernel, n_q, group, qs, keys, carried, final),
        out_shape=out_shape,
        in_specs=in_specs,
        out_specs=[vmem] * len(out_shape),
        input_output_aliases=aliases,
        cost_estimate=pl.CostEstimate(
            flops=16 * n_pairs * rows * rows * n_q * HD,
            bytes_accessed=2 * (qs[1] - qs[0]) * rows * (2 * n_q + 2 * n_kv) * HD,
            transcendentals=n_pairs * rows * rows * n_q,
        ),
        compiler_params=params(24),
        name="attend",
    )(*args)


def mix_kernel(places, n_s, n_y, n_d, index_ref, *refs):
    a_refs, w_refs = refs[:n_s], refs[n_s:-3]
    o_ref, a_held, a_whole = refs[-3:]
    _, part = a_refs[0].shape
    depth, wide = w_refs[0].shape[-2:]
    many = depth // part
    for s in range(n_s):
        a_held[index_ref[n_d + 2 * n_s + s]] = a_refs[s][...]
    for d in range(n_d):
        for p in range(many):
            at = d * depth + p * part
            a_whole[:, at : at + part] = a_held[index_ref[d] * many + p]
    for i, j in sorted({(i, j) for i, j, _ in places}):
        total = None
        for d in range(n_d):
            t, plane = places[i, j, d]
            lhs = a_whole[:, d * depth : (d + 1) * depth]
            term = jnp.dot(lhs, w_refs[t][plane], preferred_element_type=jnp.float32)
            total = term if total is None else total + term
        at = pl.multiple_of(index_ref[n_d + i * n_y + j] * wide, wide)
        o_ref[:, pl.ds(at, wide)] = total.astype(jnp.bfloat16)


def mix(heads, pieces, places, index, n_y, n_d):
    n_s = len(heads)
    rows, part = heads[0].shape
    wide = pieces[0].shape[2]
    vmem = pl.BlockSpec(memory_space=pltpu.VMEM)
    return pl.pallas_call(
        functools.partial(mix_kernel, places, n_s, n_y, n_d),
        out_shape=jax.ShapeDtypeStruct((rows, n_s * wide), jnp.bfloat16),
        in_specs=[pl.BlockSpec(memory_space=pltpu.SMEM)] + [vmem] * (n_s + len(pieces)),
        out_specs=vmem,
        scratch_shapes=[
            pltpu.VMEM((n_s, rows, part), jnp.bfloat16),
            pltpu.VMEM((rows, n_s * part), jnp.bfloat16),
        ],
        cost_estimate=pl.CostEstimate(
            flops=2 * rows * n_s * part * n_s * wide,
            bytes_accessed=2 * n_s * part * n_s * wide,
            transcendentals=0,
        ),
        compiler_params=params(16),
        name="mix",
    )(index, *heads, *pieces)


def layout(n_sp, n_dp):
    n_z, n_c = math.gcd(n_sp, 4), math.gcd(n_dp, 2)
    return n_z, n_sp // n_z, n_dp // n_c, n_c


def on_device(tokens, w_query, w_key, w_value, w_out, qk_gain):
    own_rows = tokens[0]
    rows, depth = own_rows.shape
    n_sp, n_dp = lax.axis_size("sp"), lax.axis_size("dp")
    seq_len = rows * n_sp
    n_z, n_y, n_x, n_c = layout(n_sp, n_dp)
    n_q = HQ // n_sp
    group = HQ // KV
    share = max(1, n_sp // KV)
    if share > 1:
        groups = [[g * share + i for i in range(share)] for g in range(n_sp // share)]
        whole_head = lambda w: lax.all_gather(w, "sp", axis=1, axis_index_groups=groups, tiled=True)
        w_key, w_value = whole_head(w_key), whole_head(w_value)
    n_kv = w_key.shape[1] // HD
    d_slots = [(i, 0) for i in range(n_x)] + [(i, j) for i in range(n_x) for j in range(1, n_c)]
    s_slots = [(i, j) for i in range(n_z) for j in range(n_y)]
    n_d = len(d_slots)
    last = n_z + n_y - 2
    order = sorted(s_slots, key=lambda s: max(sum(s), 1))
    s_owner = {s: owner_of("sp", n_z, n_y, *s) for s in s_slots}
    index = jnp.stack(
        [owner_of("dp", n_x, n_c, *s) for s in d_slots]
        + [s_owner[s] for s in s_slots]
        + [s_owner[s] for s in order]
        + [owner_of("sp", n_z, n_y, n_z - i, n_y - j) for i, j in order]
    ).astype(jnp.int32)
    up_z, up_y = shift(n_z, n_y, True), shift(n_z, n_y, False)
    up_x, up_c = shift(n_x, n_c, True), shift(n_x, n_c, False)

    cut = rows // 2
    blocks = {(0, 0): [own_rows[:cut], lax.optimization_barrier(own_rows)[cut:]]}
    for turn in range(1, last + 1):
        for half in range(2):
            for i, j in [s for s in s_slots if sum(s) == turn]:
                before, pairs = ((i, j - 1), up_y) if j else ((i - 1, j), up_z)
                blocks.setdefault((i, j), [None, None])[half] = lax.ppermute(
                    blocks[before][half], "sp", pairs
                )

    w_blocks = {(0, 0): jnp.concatenate([w_query, w_key, w_value], axis=1)}
    for i in range(1, n_x):
        w_blocks[i, 0] = lax.ppermute(w_blocks[i - 1, 0], "dp", up_x)
    for i in range(n_x):
        for j in range(1, n_c):
            w_blocks[i, j] = lax.ppermute(w_blocks[i, j - 1], "dp", up_c)
    weight = assemble(
        [w_blocks[s] for s in d_slots],
        [(b, None, b, None) for b in range(n_d)],
        index,
        (depth, w_blocks[0, 0].shape[1]),
    )
    tables = rotary_tables(seq_len)

    held = state = None
    n_held = n_done = 0
    for turn in range(1, last + 1):
        ready = [s for s in order if max(sum(s), 1) == turn]
        held = project(
            [blocks[s] for s in ready], [s_slots.index(s) for s in ready], n_held, weight, index, n_d,
            qk_gain, *tables, n_q, n_kv, held, n_sp,
        )
        n_held += len(ready)
        old, final = (0, n_done), turn == last
        fresh = (n_done, n_held)
        carry = functools.partial(attend, n_q=n_q, group=group)
        if n_done:
            updated = carry(held, state, old, fresh, True, final)
            state = state if final else updated
        made = carry(held, state, fresh, (0, n_held), False, final)
        if final:
            attended = [*updated, *made]
        else:
            state = made
        n_done = n_held
    heads = []
    for (i, j), block in zip(order, attended):
        if i or j:
            block = lax.ppermute(block, "sp", send_back(n_z, n_y, i, j))
        heads.append(block)

    ring = [w_out]
    for _ in range(1, n_z):
        ring.append(lax.ppermute(ring[-1], "sp", up_z))
    parts = 2 if n_z % 2 == 0 else 1
    size = n_z // parts
    pieces, places = [], {}
    for k in range(parts):
        column = jnp.stack(ring[k * size : (k + 1) * size])
        for j in range(n_y):
            if j:
                column = lax.ppermute(column, "sp", up_y)
            row = column
            for i in range(n_x):
                if i:
                    row = lax.ppermute(row, "dp", up_x)
                piece = row
                for c in range(n_c):
                    if c:
                        piece = lax.ppermute(piece, "dp", up_c)
                    for p in range(size):
                        places[k * size + p, j, d_slots.index((i, c))] = len(pieces), p
                    pieces.append(piece)
    return mix(heads, pieces, places, index, n_y, n_d)[None]


def solution(mesh):
    in_specs = (
        P("dp", "sp", None),
        P("dp", "sp"),
        P("dp", "sp"),
        P("dp", "sp"),
        P("dp", "sp"),
        P(),
    )
    out_specs = P("dp", "sp", None)

    return jax.shard_map(
        on_device, mesh=mesh, in_specs=in_specs, out_specs=out_specs, check_vma=False
    )
```

time: 418 us -> 177 us (0.42)
  waiting for transfers between devices: 273 us -> 72.7 us
  Pallas kernels: 0 us -> 44 us
  matrix products: 42.8 us -> 0 us
  blocking collectives: 30.4 us -> 0 us
  starting transfers between devices: 14.8 us -> 44.3 us
  local copies, waits for them, and re-layouts: 27.8 us -> 6.22 us
  between operations: 13.7 us -> 0.37 us
  other arithmetic: 14.5 us -> 9.26 us
    all_gather x8 -> x0, waiting for transfers between devices: 250 us -> none  [the longest x4 165 us: project(): col_full = lax.all_gather(weight, 'sp', axis=1, tiled=True)]
    ppermute x0 -> x41, waiting for transfers between devices: none -> 72.7 us  [the longest x14 49.3 us: on_device(): lax.ppermute(blocks[before][half], 'sp', pairs)]
    ppermute x0 -> x41, starting transfers between devices: none -> 44.3 us  [the longest x7 16 us: on_device(): block = lax.ppermute(block, 'sp', send_back(n_z, n_y, i, j))]
    pallas_call x0 -> x13, Pallas kernels: none -> 44 us  [the longest x7 24.5 us: attend(): pl.pallas_call(functools.partial(attend_kernel, n_q, group, qs, keys, car...]
    dot_general x20 -> x0, matrix products: 42.8 us -> none  [the longest x4 19.5 us: project(): jnp.dot(own_rows, lax.all_gather(col_full, 'dp', axis=0, tiled=True), pre...]
    all_to_all x1 -> x0, blocking collectives: 30.4 us -> none  [on_device(): lax.all_to_all(mixed_heads, 'sp', split_axis=0, concat_axis=1, tiled=True)]
    all_to_all x3 -> x0, waiting for transfers between devices: 20.1 us -> none  [the longest x1 20.1 us: on_device(): lax.all_to_all(prepare(raw_proj, qk_gain[0], cosine, sine_table).reshape(...]
    dot_general x2 -> x0, local copies, waits for them, and re-layouts: 18.7 us -> none  [project(): jnp.dot(own_rows, lax.all_gather(col_full, 'dp', axis=0, tiled=True), pre...]
  transfers between devices with their start and end apart: 11 -> 41, of which waited for: 8 -> 17; matrix products, arithmetic and copies ran while one was open for 19% -> 9% of each run, Pallas kernels for 0% -> 22%
where the time goes in v1:
time: 177 us
  waiting for transfers between devices  72.7 us (41%)
  starting transfers between devices  44.3 us (25%)
  Pallas kernels  44 us (25%)
  other arithmetic  9.26 us (5%)
  local copies, waits for them, and re-layouts  6.22 us (4%)
    ppermute x14, waiting for transfers between devices, on_device(): lax.ppermute(blocks[before][half], 'sp', pairs)  49.3 us
    pallas_call x7, Pallas kernels, attend(): pl.pallas_call(functools.partial(attend_kernel, n_q, group, qs, keys, car...  24.5 us
    ppermute x7, starting transfers between devices, on_device(): block = lax.ppermute(block, 'sp', send_back(n_z, n_y, i, j))  16 us
    pallas_call x4, Pallas kernels, project(): pl.pallas_call(functools.partial(project_kernel, n_b, n_x, n_q, n_kv, fir...  14.1 us
    ppermute x14, starting transfers between devices, on_device(): lax.ppermute(blocks[before][half], 'sp', pairs)  13 us
    ppermute x7, waiting for transfers between devices, on_device(): block = lax.ppermute(block, 'sp', send_back(n_z, n_y, i, j))  11.9 us
    ppermute x3, waiting for transfers between devices, on_device(): ring.append(lax.ppermute(ring[-1], 'sp', up_z))  6.07 us
    mul x1, other arithmetic, rotary_tables(): return (jnp.cos(angle), jnp.sin(angle) * sign)  5.19 us
  transfers between devices with their start and end apart: 41, of which 17 were waited for; matrix products, arithmetic and copies ran while one was open for 9% of the time, Pallas kernels for 22%

profile of v1, /device:TPU:0, one launch (start us, length us, event | category | flops | bytes accessed | tf_op | source)
XLA Modules:
  0.0 176.9 jit_solution(1782771229457998726)
XLA Ops:
  0.0 3.1 %collective-permute-start.24 = (bf16[512,256]{1,0:T(8,128)(2,1)}, bf16[512,256]{1,0:T(8,128)(2,1)S(1)}, u32[]{:S(2)}, u32[]{:S(2)}) collective-permute-start(bf16[512,256]{1,0:T(8,128)(2,1)} %param.10), channel_id=1, source_target_pairs={{0,8},{4,12},{8,16},{12,20},{16,24},{20,28},{24,0},{28,4},{1,9},{5... | collective-permute-start | bytes 786440 | tf_op jit(solution)/shard_map/ppermute | solution.py:398
  7.5 4.1 %collective-permute-done.24 = bf16[512,256]{1,0:T(8,128)(2,1)S(1)} collective-permute-done((bf16[512,256]{1,0:T(8,128)(2,1)}, bf16[512,256]{1,0:T(8,128)(2,1)S(1)}, u32[]{:S(2)}, u32[]{:S(2)}) %collective-permute-start.24) | collective-permute-done | bytes 262176 | tf_op jit(solution)/shard_map/ppermute | solution.py:398
  27.0 6.8 %collective-permute-done.refs_4_ = bf16[128,2048]{1,0:T(8,128)(2,1)S(1)} collective-permute-done((bf16[128,2048]{1,0:T(8,128)(2,1)S(1)}, bf16[128,2048]{1,0:T(8,128)(2,1)S(1)}, u32[]{:S(2)}, u32[]{:S(2)}) %collective-permute-start) | collective-permute-done | bytes 524320 | tf_op jit(solution)/shard_map/ppermute | solution.py:351
  35.3 9.7 %collective-permute-done.4.refs_5_ = bf16[128,2048]{1,0:T(8,128)(2,1)S(1)} collective-permute-done((bf16[128,2048]{1,0:T(8,128)(2,1)}, bf16[128,2048]{1,0:T(8,128)(2,1)S(1)}, u32[]{:S(2)}, u32[]{:S(2)}) %collective-permute-start.4) | collective-permute-done | bytes 524320 | tf_op jit(solution)/shard_map/ppermute | solution.py:351
  49.1 5.2 %sine_multiply_fusion = (f32[2048,128]{1,0:T(8,128)S(1)}, f32[2048,128]{1,0:T(8,128)S(1)}) fusion(f32[128]{0:T(128)S(1)} %compare_select_fusion, f32[2048,64]{1,0:T(8,128)} %get-tuple-element.66, f32[2048,64]{1,0:T(8,128)} %get-tuple-element.65), kind=kLoop, calls=%fused_computation.1 | loop fusion | flops 524288 | bytes 3146240 | tf_op jit(solution)/shard_map/mul | solution.py:30
  59.7 6.2 %collective-permute-done.1.refs_2_ = bf16[128,2048]{1,0:T(8,128)(2,1)S(1)} collective-permute-done((bf16[128,2048]{1,0:T(8,128)(2,1)}, bf16[128,2048]{1,0:T(8,128)(2,1)S(1)}, u32[]{:S(2)}, u32[]{:S(2)}) %collective-permute-start.1) | collective-permute-done | bytes 524320 | tf_op jit(solution)/shard_map/ppermute | solution.py:351
  65.9 5.5 %project.4 = (bf16[8,256,256]{2,1,0:T(8,128)(2,1)S(1)}, bf16[8,256,128]{2,1,0:T(8,128)(2,1)S(1)}, bf16[8,256,128]{2,1,0:T(8,128)(2,1)S(1)}) custom-call(s32[28]{0:T(128)S(1)} %stack.100.index_ref, bf16[128,2048]{1,0:T(8,128)(2,1)S(1)} %slice_bitcast_fusion.refs_0_, bf16[128,2048]{1,0:T(8,128)(2,1)} %slice.12.refs_1_, ...), custom_call_target="tpu_custom_call" | custom-call | flops 3221225472 | bytes 6029312 | tf_op jit(solution)/shard_map/project/pallas_call | solution.py:162
  71.3 5.7 %collective-permute-done.5.refs_3_ = bf16[128,2048]{1,0:T(8,128)(2,1)S(1)} collective-permute-done((bf16[128,2048]{1,0:T(8,128)(2,1)S(1)}, bf16[128,2048]{1,0:T(8,128)(2,1)S(1)}, u32[]{:S(2)}, u32[]{:S(2)}) %collective-permute-start.5) | collective-permute-done | bytes 524320 | tf_op jit(solution)/shard_map/ppermute | solution.py:351
  81.7 3.0 %attend.7 = (f32[8,256,256]{2,1,0:T(8,128)S(1)}, f32[8,256,128]{2,1,0:T(8,128)S(1)}) custom-call(bf16[8,256,256]{2,1,0:T(8,128)(2,1)S(1)} %get-tuple-element.34.refs_10_.q_ref, bf16[8,256,128]{2,1,0:T(8,128)(2,1)S(1)} %get-tuple-element.35.refs_11_.k_ref, bf16[8,256,128]{2,1,0:T(8,128)(2,1)S(1)} %get-tuple-element.36.refs_12_.v_ref), custom_call_target="tpu_custom_call" | custom-call | flops 2415919104 | bytes 1179648 | tf_op jit(solution)/shard_map/attend/pallas_call | solution.py:248
  84.7 3.2 %project.5 = (bf16[8,256,256]{2,1,0:T(8,128)(2,1)S(1)}, bf16[8,256,128]{2,1,0:T(8,128)(2,1)S(1)}, bf16[8,256,128]{2,1,0:T(8,128)(2,1)S(1)}) custom-call(s32[28]{0:T(128)S(1)} %stack.100.index_ref, bf16[128,2048]{1,0:T(8,128)(2,1)S(1)} %collective-permute-done.13.refs_0_, ...), custom_call_target="tpu_custom_call", output_to_operand_aliasing={{0}: (11, {}), {1}: (12, {}), {2}: (13, {})} | custom-call | flops 2147483648 | bytes 4718592 | tf_op jit(solution)/shard_map/project/pallas_call | solution.py:162
  87.9 3.7 %collective-permute-done.37.refs_20_ = bf16[2,512,256]{2,1,0:T(8,128)(2,1)S(1)} collective-permute-done((bf16[2,512,256]{2,1,0:T(8,128)(2,1)S(1)}, bf16[2,512,256]{2,1,0:T(8,128)(2,1)S(1)}, u32[]{:S(2)}, u32[]{:S(2)}) %collective-permute-start.37) | collective-permute-done | bytes 524320 | tf_op jit(solution)/shard_map/ppermute | solution.py:406
  92.9 3.0 %attend.8 = (f32[8,256,256]{2,1,0:T(8,128)S(1)}, f32[8,256,128]{2,1,0:T(8,128)S(1)}) custom-call(bf16[8,256,256]{2,1,0:T(8,128)(2,1)S(1)} %get-tuple-element.37.refs_10_.q_ref, bf16[8,256,128]{2,1,0:T(8,128)(2,1)S(1)} %get-tuple-element.38.refs_11_.k_ref, ...), custom_call_target="tpu_custom_call", output_to_operand_aliasing={{0}: (3, {}), {1}: (4, {})} | custom-call | flops 1610612736 | bytes 1179648 | tf_op jit(solution)/shard_map/attend/pallas_call | solution.py:248
  98.1 4.8 %collective-permute-done.11.refs_0_ = bf16[128,2048]{1,0:T(8,128)(2,1)S(1)} collective-permute-done((bf16[128,2048]{1,0:T(8,128)(2,1)S(1)}, bf16[128,2048]{1,0:T(8,128)(2,1)S(1)}, u32[]{:S(2)}, u32[]{:S(2)}) %collective-permute-start.11) | collective-permute-done | bytes 524320 | tf_op jit(solution)/shard_map/ppermute | solution.py:351
  102.9 8.7 %collective-permute-done.12.refs_1_ = bf16[128,2048]{1,0:T(8,128)(2,1)S(1)} collective-permute-done((bf16[128,2048]{1,0:T(8,128)(2,1)S(1)}, bf16[128,2048]{1,0:T(8,128)(2,1)S(1)}, u32[]{:S(2)}, u32[]{:S(2)}) %collective-permute-start.12) | collective-permute-done | bytes 524320 | tf_op jit(solution)/shard_map/ppermute | solution.py:351
  115.8 3.2 %project.6 = (bf16[8,256,256]{2,1,0:T(8,128)(2,1)S(1)}, bf16[8,256,128]{2,1,0:T(8,128)(2,1)S(1)}, bf16[8,256,128]{2,1,0:T(8,128)(2,1)S(1)}) custom-call(s32[28]{0:T(128)S(1)} %stack.100.index_ref, bf16[128,2048]{1,0:T(8,128)(2,1)S(1)} %collective-permute-done.11.refs_0_, ...), custom_call_target="tpu_custom_call", output_to_operand_aliasing={{0}: (11, {}), {1}: (12, {}), {2}: (13, {})} | custom-call | flops 2147483648 | bytes 4718592 | tf_op jit(solution)/shard_map/project/pallas_call | solution.py:162
  120.7 5.1 %attend.10 = (f32[8,256,256]{2,1,0:T(8,128)S(1)}, f32[8,256,128]{2,1,0:T(8,128)S(1)}) custom-call(bf16[8,256,256]{2,1,0:T(8,128)(2,1)S(1)} %get-tuple-element.40.refs_6_.q_ref, bf16[8,256,128]{2,1,0:T(8,128)(2,1)S(1)} %get-tuple-element.41.refs_7_.k_ref, ...), custom_call_target="tpu_custom_call", output_to_operand_aliasing={{0}: (3, {}), {1}: (4, {})} | custom-call | flops 2684354560 | bytes 1966080 | tf_op jit(solution)/shard_map/attend/pallas_call | solution.py:248
  126.4 3.4 %attend.11 = (f32[8,256,256]{2,1,0:T(8,128)S(1)}, f32[8,256,128]{2,1,0:T(8,128)S(1)}) custom-call(bf16[8,256,256]{2,1,0:T(8,128)(2,1)S(1)} %get-tuple-element.40.refs_6_.q_ref, bf16[8,256,128]{2,1,0:T(8,128)(2,1)S(1)} %get-tuple-element.41.refs_7_.k_ref, ...), custom_call_target="tpu_custom_call", output_to_operand_aliasing={{0}: (3, {}), {1}: (4, {})} | custom-call | flops 3758096384 | bytes 786432 | tf_op jit(solution)/shard_map/attend/pallas_call | solution.py:248
  129.8 4.4 %collective-permute-done.7.refs_1_ = bf16[128,2048]{1,0:T(8,128)(2,1)S(1)} collective-permute-done((bf16[128,2048]{1,0:T(8,128)(2,1)S(1)}, bf16[128,2048]{1,0:T(8,128)(2,1)S(1)}, u32[]{:S(2)}, u32[]{:S(2)}) %collective-permute-start.7) | collective-permute-done | bytes 524320 | tf_op jit(solution)/shard_map/ppermute | solution.py:351
  137.0 5.5 %attend.12 = (bf16[256,256]{1,0:T(8,128)(2,1)S(1)}, bf16[256,256]{1,0:T(8,128)(2,1)S(1)}, bf16[256,256]{1,0:T(8,128)(2,1)S(1)}, bf16[256,256]{1,0:T(8,128)(2,1)S...) custom-call(bf16[8,256,256]{2,1,0:T(8,128)(2,1)S(1)} %get-tuple-element.43.q_ref, ...), custom_call_target="tpu_custom_call" | custom-call | flops 1879048192 | bytes 2752512 | tf_op jit(solution)/shard_map/attend/pallas_call | solution.py:248
  146.2 3.5 %collective-permute-start.18 = (bf16[256,256]{1,0:T(8,128)(2,1)S(1)}, bf16[256,256]{1,0:T(8,128)(2,1)S(1)}, u32[]{:S(2)}, u32[]{:S(2)}) collective-permute-start(bf16[256,256]{1,0:T(8,128)(2,1)S(1)} %get-tuple-element.58), channel_id=1, source_target_pairs={{0,24},{4,28},{8,0},{12,4},{16,8},{20,12},{24,16},{28,20},{1,25},{... | collective-permute-start | bytes 393224 | tf_op jit(solution)/shard_map/ppermute | solution.py:393
  152.7 4.5 %collective-permute-start.20 = (bf16[256,256]{1,0:T(8,128)(2,1)S(1)}, bf16[256,256]{1,0:T(8,128)(2,1)S(1)}, u32[]{:S(2)}, u32[]{:S(2)}) collective-permute-start(bf16[256,256]{1,0:T(8,128)(2,1)S(1)} %get-tuple-element.60), channel_id=1, source_target_pairs={{0,16},{4,20},{8,24},{12,28},{16,0},{20,4},{24,8},{28,12},{1,17},{... | collective-permute-start | bytes 393224 | tf_op jit(solution)/shard_map/ppermute | solution.py:393
  157.5 3.3 %collective-permute-start.22 = (bf16[256,256]{1,0:T(8,128)(2,1)S(1)}, bf16[256,256]{1,0:T(8,128)(2,1)S(1)}, u32[]{:S(2)}, u32[]{:S(2)}) collective-permute-start(bf16[256,256]{1,0:T(8,128)(2,1)S(1)} %get-tuple-element.62), channel_id=1, source_target_pairs={{0,8},{4,12},{8,16},{12,20},{16,24},{20,28},{24,0},{28,4},{1,9},{5... | collective-permute-start | bytes 393224 | tf_op jit(solution)/shard_map/ppermute | solution.py:393
  160.8 8.9 %collective-permute-done.20.refs_4_ = bf16[256,256]{1,0:T(8,128)(2,1)S(1)} collective-permute-done((bf16[256,256]{1,0:T(8,128)(2,1)S(1)}, bf16[256,256]{1,0:T(8,128)(2,1)S(1)}, u32[]{:S(2)}, u32[]{:S(2)}) %collective-permute-start.20) | collective-permute-done | bytes 131104 | tf_op jit(solution)/shard_map/ppermute | solution.py:393
  172.2 4.7 %mix.1 = bf16[256,2048]{1,0:T(8,128)(2,1)} custom-call(s32[28]{0:T(128)S(1)} %stack.100.index_ref, bf16[256,256]{1,0:T(8,128)(2,1)S(1)} %get-tuple-element.56.refs_0_, bf16[256,256]{1,0:T(8,128)(2,1)S(1)} %collective-permute-done.17.refs_1_, bf16[256,256]{1,0:T(8,128)(2,1)S(1)} %collective-permute-done.18.refs_2_, ...), custom_call_target="tpu_custom_call" | custom-call | flops 2147483648 | bytes 8388608 | tf_op jit(solution)/shard_map/mix/pallas_call | solution.py:292
  (100 shorter events, 57.5 us)
Async XLA Ops:
  12.8 21.0 %collective-permute-start = (bf16[128,2048]{1,0:T(8,128)(2,1)S(1)}, bf16[128,2048]{1,0:T(8,128)(2,1)S(1)}, u32[]{:S(2)}, u32[]{:S(2)}) collective-permute-start(bf16[128,2048]{1,0:T(8,128)(2,1)S(1)} %slice_bitcast_fusion.refs_0_), channel_id=1, source_target_pairs={{0,8},{4,12},{8,16},{12,20},{16,24},{20,28},{24,0},{28,4},{1,9},{5... | collective-permute-start | bytes 1572872 | tf_op jit(solution)/shard_map/ppermute | solution.py:351
  14.0 32.5 %collective-permute-start.15 = (bf16[128,2048]{1,0:T(8,128)(2,1)S(1)}, bf16[128,2048]{1,0:T(8,128)(2,1)}, u32[]{:S(2)}, u32[]{:S(2)}) collective-permute-start(bf16[128,2048]{1,0:T(8,128)(2,1)S(1)} %slice_bitcast_fusion.refs_0_), channel_id=1, source_target_pairs={{0,4},{4,0},{8,12},{12,8},{16,20},{20,16},{24,28},{28,24},{1,5},{5... | collective-permute-start | bytes 1572872 | tf_op jit(solution)/shard_map/ppermute | solution.py:351
  19.4 25.7 %collective-permute-start.4 = (bf16[128,2048]{1,0:T(8,128)(2,1)}, bf16[128,2048]{1,0:T(8,128)(2,1)S(1)}, u32[]{:S(2)}, u32[]{:S(2)}) collective-permute-start(bf16[128,2048]{1,0:T(8,128)(2,1)} %slice.12.refs_1_), channel_id=1, source_target_pairs={{0,8},{4,12},{8,16},{12,20},{16,24},{20,28},{24,0},{28,4},{1,9},{5... | collective-permute-start | bytes 1572872 | tf_op jit(solution)/shard_map/ppermute | solution.py:351
  20.9 25.9 %collective-permute-start.16 = (bf16[128,2048]{1,0:T(8,128)(2,1)}, bf16[128,2048]{1,0:T(8,128)(2,1)}, u32[]{:S(2)}, u32[]{:S(2)}) collective-permute-start(bf16[128,2048]{1,0:T(8,128)(2,1)} %slice.12.refs_1_), channel_id=1, source_target_pairs={{0,4},{4,0},{8,12},{12,8},{16,20},{20,16},{24,28},{28,24},{1,5},{5... | collective-permute-start | bytes 1572872 | tf_op jit(solution)/shard_map/ppermute | solution.py:351
  22.7 26.4 %collective-permute-start.33 = (bf16[512,256]{1,0:T(8,128)(2,1)}, bf16[512,256]{1,0:T(8,128)(2,1)}, u32[]{:S(2)}, u32[]{:S(2)}) collective-permute-start(bf16[512,256]{1,0:T(8,128)(2,1)} %collective-permute-done.32), channel_id=1, source_target_pairs={{0,8},{4,12},{8,16},{12,20},{16,24},{20,28},{24,0},{28,4},{1,9},{5... | collective-permute-start | bytes 786440 | tf_op jit(solution)/shard_map/ppermute | solution.py:398
  33.8 20.5 %collective-permute-start.28 = (bf16[2,512,256]{2,1,0:T(8,128)(2,1)S(1)}, bf16[2,512,256]{2,1,0:T(8,128)(2,1)}, u32[]{:S(2)}, u32[]{:S(2)}) collective-permute-start(bf16[2,512,256]{2,1,0:T(8,128)(2,1)S(1)} %pad_maximum_fusion.1.refs_8_), channel_id=1, source_target_pairs={{0,4},{4,0},{8,12},{12,8},{16,20},{20,16},{24,28},{28,24},{1,5},{5... | collective-permute-start | bytes 1572872 | tf_op jit(solution)/shard_map/ppermute | solution.py:406
  54.3 24.1 %collective-permute-start.13 = (bf16[128,2048]{1,0:T(8,128)(2,1)S(1)}, bf16[128,2048]{1,0:T(8,128)(2,1)S(1)}, u32[]{:S(2)}, u32[]{:S(2)}) collective-permute-start(bf16[128,2048]{1,0:T(8,128)(2,1)S(1)} %copy-done.2), channel_id=1, source_target_pairs={{0,4},{4,0},{8,12},{12,8},{16,20},{20,16},{24,28},{28,24},{1,5},{5... | collective-permute-start | bytes 1572872 | tf_op jit(solution)/shard_map/ppermute | solution.py:351
  55.7 21.4 %collective-permute-start.5 = (bf16[128,2048]{1,0:T(8,128)(2,1)S(1)}, bf16[128,2048]{1,0:T(8,128)(2,1)S(1)}, u32[]{:S(2)}, u32[]{:S(2)}) collective-permute-start(bf16[128,2048]{1,0:T(8,128)(2,1)S(1)} %copy-done.4), channel_id=1, source_target_pairs={{0,8},{4,12},{8,16},{12,20},{16,24},{20,28},{24,0},{28,4},{1,9},{5... | collective-permute-start | bytes 1572872 | tf_op jit(solution)/shard_map/ppermute | solution.py:351
  55.7 24.7 %collective-permute-start.14 = (bf16[128,2048]{1,0:T(8,128)(2,1)S(1)}, bf16[128,2048]{1,0:T(8,128)(2,1)S(1)}, u32[]{:S(2)}, u32[]{:S(2)}) collective-permute-start(bf16[128,2048]{1,0:T(8,128)(2,1)S(1)} %copy-done.4), channel_id=1, source_target_pairs={{0,4},{4,0},{8,12},{12,8},{16,20},{20,16},{24,28},{28,24},{1,5},{5... | collective-permute-start | bytes 1572872 | tf_op jit(solution)/shard_map/ppermute | solution.py:351
  58.7 32.9 %collective-permute-start.37 = (bf16[2,512,256]{2,1,0:T(8,128)(2,1)S(1)}, bf16[2,512,256]{2,1,0:T(8,128)(2,1)S(1)}, u32[]{:S(2)}, u32[]{:S(2)}) collective-permute-start(bf16[2,512,256]{2,1,0:T(8,128)(2,1)S(1)} %pad_maximum_fusion.2.refs_16_), channel_id=1, source_target_pairs={{0,4},{4,0},{8,12},{12,8},{16,20},{20,16},{24,28},{28,24},{1,5},{5... | collective-permute-start | bytes 1572872 | tf_op jit(solution)/shard_map/ppermute | solution.py:406
  65.9 27.0 %collective-permute-start.2 = (bf16[128,2048]{1,0:T(8,128)(2,1)S(1)}, bf16[128,2048]{1,0:T(8,128)(2,1)S(1)}, u32[]{:S(2)}, u32[]{:S(2)}) collective-permute-start(bf16[128,2048]{1,0:T(8,128)(2,1)S(1)} %collective-permute-done.1.refs_2_), channel_id=1, source_target_pairs={{0,8},{4,12},{8,16},{12,20},{16,24},{20,28},{24,0},{28,4},{1,9},{5... | collective-permute-start | bytes 1572872 | tf_op jit(solution)/shard_map/ppermute | solution.py:351
  77.1 25.8 %collective-permute-start.11 = (bf16[128,2048]{1,0:T(8,128)(2,1)S(1)}, bf16[128,2048]{1,0:T(8,128)(2,1)S(1)}, u32[]{:S(2)}, u32[]{:S(2)}) collective-permute-start(bf16[128,2048]{1,0:T(8,128)(2,1)S(1)} %collective-permute-done.1.refs_2_), channel_id=1, source_target_pairs={{0,4},{4,0},{8,12},{12,8},{16,20},{20,16},{24,28},{28,24},{1,5},{5... | collective-permute-start | bytes 1572872 | tf_op jit(solution)/shard_map/ppermute | solution.py:351
  78.4 18.6 %collective-permute-start.6 = (bf16[128,2048]{1,0:T(8,128)(2,1)S(1)}, bf16[128,2048]{1,0:T(8,128)(2,1)S(1)}, u32[]{:S(2)}, u32[]{:S(2)}) collective-permute-start(bf16[128,2048]{1,0:T(8,128)(2,1)S(1)} %collective-permute-done.5.refs_3_), channel_id=1, source_target_pairs={{0,8},{4,12},{8,16},{12,20},{16,24},{20,28},{24,0},{28,4},{1,9},{5... | collective-permute-start | bytes 1572872 | tf_op jit(solution)/shard_map/ppermute | solution.py:351
  80.4 31.1 %collective-permute-start.12 = (bf16[128,2048]{1,0:T(8,128)(2,1)S(1)}, bf16[128,2048]{1,0:T(8,128)(2,1)S(1)}, u32[]{:S(2)}, u32[]{:S(2)}) collective-permute-start(bf16[128,2048]{1,0:T(8,128)(2,1)S(1)} %collective-permute-done.5.refs_3_), channel_id=1, source_target_pairs={{0,4},{4,0},{8,12},{12,8},{16,20},{20,16},{24,28},{28,24},{1,5},{5... | collective-permute-start | bytes 1572872 | tf_op jit(solution)/shard_map/ppermute | solution.py:351
  91.6 27.3 %collective-permute-start.35 = (bf16[2,512,256]{2,1,0:T(8,128)(2,1)S(1)}, bf16[2,512,256]{2,1,0:T(8,128)(2,1)S(1)}, u32[]{:S(2)}, u32[]{:S(2)}) collective-permute-start(bf16[2,512,256]{2,1,0:T(8,128)(2,1)S(1)} %pad_maximum_fusion.2.refs_16_), channel_id=1, source_target_pairs={{0,2},{1,3},{2,0},{3,1},{4,6},{5,7},{6,4},{7,5},{8,10},{9,11},{10,... | collective-permute-start | bytes 1572872 | tf_op jit(solution)/shard_map/ppermute | solution.py:410
  92.9 27.3 %collective-permute-start.34 = (bf16[2,512,256]{2,1,0:T(8,128)(2,1)S(1)}, bf16[2,512,256]{2,1,0:T(8,128)(2,1)S(1)}, u32[]{:S(2)}, u32[]{:S(2)}) collective-permute-start(bf16[2,512,256]{2,1,0:T(8,128)(2,1)S(1)} %pad_maximum_fusion.2.refs_16_), channel_id=1, source_target_pairs={{0,1},{1,0},{2,3},{3,2},{4,5},{5,4},{6,7},{7,6},{8,9},{9,8},{10,11... | collective-permute-start | bytes 1572872 | tf_op jit(solution)/shard_map/ppermute | solution.py:414
  97.0 28.7 %collective-permute-start.30 = (bf16[2,512,256]{2,1,0:T(8,128)(2,1)}, bf16[2,512,256]{2,1,0:T(8,128)(2,1)S(1)}, u32[]{:S(2)}, u32[]{:S(2)}) collective-permute-start(bf16[2,512,256]{2,1,0:T(8,128)(2,1)} %collective-permute-done.28.refs_12_), channel_id=1, source_target_pairs={{0,2},{1,3},{2,0},{3,1},{4,6},{5,7},{6,4},{7,5},{8,10},{9,11},{10,... | collective-permute-start | bytes 1572872 | tf_op jit(solution)/shard_map/ppermute | solution.py:410
  102.9 23.0 %collective-permute-start.29 = (bf16[2,512,256]{2,1,0:T(8,128)(2,1)}, bf16[2,512,256]{2,1,0:T(8,128)(2,1)S(1)}, u32[]{:S(2)}, u32[]{:S(2)}) collective-permute-start(bf16[2,512,256]{2,1,0:T(8,128)(2,1)} %collective-permute-done.28.refs_12_), channel_id=1, source_target_pairs={{0,1},{1,0},{2,3},{3,2},{4,5},{5,4},{6,7},{7,6},{8,9},{9,8},{10,11... | collective-permute-start | bytes 1572872 | tf_op jit(solution)/shard_map/ppermute | solution.py:414
  119.0 17.4 %collective-permute-start.39 = (bf16[2,512,256]{2,1,0:T(8,128)(2,1)S(1)}, bf16[2,512,256]{2,1,0:T(8,128)(2,1)S(1)}, u32[]{:S(2)}, u32[]{:S(2)}) collective-permute-start(bf16[2,512,256]{2,1,0:T(8,128)(2,1)S(1)} %collective-permute-done.37.refs_20_), channel_id=1, source_target_pairs={{0,2},{1,3},{2,0},{3,1},{4,6},{5,7},{6,4},{7,5},{8,10},{9,11},{10,... | collective-permute-start | bytes 1572872 | tf_op jit(solution)/shard_map/ppermute | solution.py:410
  125.7 18.6 %collective-permute-start.27 = (bf16[2,512,256]{2,1,0:T(8,128)(2,1)}, bf16[2,512,256]{2,1,0:T(8,128)(2,1)S(1)}, u32[]{:S(2)}, u32[]{:S(2)}) collective-permute-start(bf16[2,512,256]{2,1,0:T(8,128)(2,1)} %collective-permute-done.26.refs_10_), channel_id=1, source_target_pairs={{0,1},{1,0},{2,3},{3,2},{4,5},{5,4},{6,7},{7,6},{8,9},{9,8},{10,11... | collective-permute-start | bytes 1572872 | tf_op jit(solution)/shard_map/ppermute | solution.py:414
  125.8 18.7 %collective-permute-start.38 = (bf16[2,512,256]{2,1,0:T(8,128)(2,1)S(1)}, bf16[2,512,256]{2,1,0:T(8,128)(2,1)S(1)}, u32[]{:S(2)}, u32[]{:S(2)}) collective-permute-start(bf16[2,512,256]{2,1,0:T(8,128)(2,1)S(1)} %collective-permute-done.37.refs_20_), channel_id=1, source_target_pairs={{0,1},{1,0},{2,3},{3,2},{4,5},{5,4},{6,7},{7,6},{8,9},{9,8},{10,11... | collective-permute-start | bytes 1572872 | tf_op jit(solution)/shard_map/ppermute | solution.py:414
  126.3 19.8 %collective-permute-start.36 = (bf16[2,512,256]{2,1,0:T(8,128)(2,1)S(1)}, bf16[2,512,256]{2,1,0:T(8,128)(2,1)S(1)}, u32[]{:S(2)}, u32[]{:S(2)}) collective-permute-start(bf16[2,512,256]{2,1,0:T(8,128)(2,1)S(1)} %collective-permute-done.35.refs_18_), channel_id=1, source_target_pairs={{0,1},{1,0},{2,3},{3,2},{4,5},{5,4},{6,7},{7,6},{8,9},{9,8},{10,11... | collective-permute-start | bytes 1572872 | tf_op jit(solution)/shard_map/ppermute | solution.py:414
  136.4 35.8 %collective-permute-start.40 = (bf16[2,512,256]{2,1,0:T(8,128)(2,1)S(1)}, bf16[2,512,256]{2,1,0:T(8,128)(2,1)S(1)}, u32[]{:S(2)}, u32[]{:S(2)}) collective-permute-start(bf16[2,512,256]{2,1,0:T(8,128)(2,1)S(1)} %collective-permute-done.39.refs_22_), channel_id=1, source_target_pairs={{0,1},{1,0},{2,3},{3,2},{4,5},{5,4},{6,7},{7,6},{8,9},{9,8},{10,11... | collective-permute-start | bytes 1572872 | tf_op jit(solution)/shard_map/ppermute | solution.py:414
  152.7 17.0 %collective-permute-start.20 = (bf16[256,256]{1,0:T(8,128)(2,1)S(1)}, bf16[256,256]{1,0:T(8,128)(2,1)S(1)}, u32[]{:S(2)}, u32[]{:S(2)}) collective-permute-start(bf16[256,256]{1,0:T(8,128)(2,1)S(1)} %get-tuple-element.60), channel_id=1, source_target_pairs={{0,16},{4,20},{8,24},{12,28},{16,0},{20,4},{24,8},{28,12},{1,17},{... | collective-permute-start | bytes 393224 | tf_op jit(solution)/shard_map/ppermute | solution.py:393
  (24 other events, 284.1 us)

commit v2 on v1

--- a/solution.py
+++ b/solution.py
@@ -108,18 +108,21 @@
     gain_ref, w_ref = refs[:2]
     outs, held, x_whole, x_sem, sem = refs[-9:-6], refs[-6:-3], refs[-3], refs[-2], refs[-1]
     q_ref, k_ref, v_ref = held
-    loads = []
+    loads, ends, at = [], [], 0
     for t in range(n_x):
         height = x_refs[t].shape[0]
-        loads.append(pltpu.make_async_copy(x_refs[t], x_whole.at[pl.ds(t * height, height)], x_sem.at[t]))
+        loads.append(pltpu.make_async_copy(x_refs[t], x_whole.at[pl.ds(at, height)], x_sem.at[t]))
         loads[-1].start()
+        at += height
+        ends.append(at)
     q_width, kv_width = n_q * HD, n_kv * HD
     even = lax.broadcasted_iota(jnp.int32, cos_refs[0].shape, 1) % 2 == 0
     rows = q_ref.shape[1]
     copies = []
     for b in range(n_b):
-        for load in loads[b * n_x // n_b : (b + 1) * n_x // n_b]:
-            load.wait()
+        while ends and ends[0] <= (b + 1) * rows:
+            ends.pop(0)
+            loads.pop(0).wait()
         x = x_whole[b * rows : (b + 1) * rows, :]
         total = jnp.dot(x, w_ref[...], preferred_element_type=jnp.float32)
         cos, sin = cos_refs[b][...], sin_refs[b][...]
@@ -148,7 +151,7 @@
     halves = [half for block in blocks for half in block]
     n_b, n_x = len(blocks), len(halves)
     depth = halves[0].shape[1]
-    rows = halves[0].shape[0] * n_x // n_b
+    rows = sum(half.shape[0] for half in halves) // n_b
     width = weight.shape[1]
     at_rows = [pl.BlockSpec((rows, HD), lambda i, ix, s=s: (ix[n_d + s], 0)) for s in slots]
     in_specs = [ANY] * n_x + at_rows + at_rows + [whole(gain.shape), whole(weight.shape)]
@@ -187,37 +190,45 @@
 
 def attend_kernel(n_q, group, qs, keys, carried, final, q_ref, k_ref, v_ref, *refs):
     if carried:
-        acc_in, ml_in = refs[:2]
+        acc_old, top_old = refs[:2]
     outs = refs[-(qs[1] - qs[0]) :] if final else refs[-2:]
     rows = q_ref.shape[1]
     scale = HD**-0.5 * LOG2E
+
+    n_keys = (keys[1] - keys[0]) * rows
+    ones = jnp.ones((n_keys, HD), jnp.bfloat16)
 
     def one(b, out_ref):
         for h in range(n_q):
             at = (h // group) * HD
             cols = slice(h * HD, (h + 1) * HD)
-            some = k_ref[keys[0] : keys[1], :, at : at + HD].reshape((keys[1] - keys[0]) * rows, HD)
-            values = v_ref[keys[0] : keys[1], :, at : at + HD].reshape((keys[1] - keys[0]) * rows, HD)
+            both = slice(2 * h * HD, 2 * (h + 1) * HD)
+            some = k_ref[keys[0] : keys[1], :, at : at + HD].reshape(n_keys, HD)
+            values = v_ref[keys[0] : keys[1], :, at : at + HD].reshape(n_keys, HD)
             scores = lax.dot_general(
                 q_ref[b, :, cols], some, (((1,), (1,)), ((), ())), preferred_element_type=jnp.float32
             )
-            top = jnp.max(scores, axis=1, keepdims=True)
+            top = jnp.broadcast_to(jnp.max(scores, axis=1, keepdims=True), (rows, HD))
             if carried:
-                top_in = ml_in[b, :, 2 * h : 2 * h + 1]
+                top_in = top_old[b, :, cols]
                 top = jnp.maximum(top, top_in)
+            weights = [
+                jnp.exp2((scores[:, c : c + HD] - top) * scale).astype(jnp.bfloat16)
+                for c in range(0, n_keys, HD)
+            ]
+            out = jnp.dot(
+                jnp.concatenate(weights, axis=1),
+                jnp.concatenate([values, ones], axis=1),
+                preferred_element_type=jnp.float32,
+            )
+            if carried:
                 fade = jnp.exp2((top_in - top) * scale)
-            weights = jnp.exp2((scores - top) * scale)
-            total = jnp.sum(weights, axis=1, keepdims=True)
-            out = jnp.dot(weights.astype(jnp.bfloat16), values, preferred_element_type=jnp.float32)
-            if carried:
-                total = total + fade * ml_in[b, :, 2 * h + 1 : 2 * h + 2]
-                out = out + fade * acc_in[b, :, cols]
+                out = out + jnp.concatenate([fade, fade], axis=1) * acc_old[b, :, both]
             if final:
-                out_ref[:, cols] = (out * (1.0 / total)).astype(jnp.bfloat16)
+                out_ref[:, cols] = (out[:, :HD] * (1.0 / out[:, HD:])).astype(jnp.bfloat16)
             else:
-                outs[0][b, :, cols] = out
-                outs[1][b, :, 2 * h : 2 * h + 1] = top
-                outs[1][b, :, 2 * h + 1 : 2 * h + 2] = total
+                outs[0][b, :, both] = out
+                outs[1][b, :, cols] = top
 
     if final:
         for b in range(*qs):
@@ -239,8 +250,8 @@
         out_shape = [jax.ShapeDtypeStruct((rows, n_q * HD), jnp.bfloat16)] * (qs[1] - qs[0])
     else:
         out_shape = [
+            jax.ShapeDtypeStruct((n_all, rows, 2 * n_q * HD), jnp.float32),
             jax.ShapeDtypeStruct((n_all, rows, n_q * HD), jnp.float32),
-            jax.ShapeDtypeStruct((n_all, rows, 128), jnp.float32),
         ]
         if state is not None:
             aliases = {3: 0, 4: 1}
@@ -261,51 +272,71 @@
     )(*args)
 
 
-def mix_kernel(places, n_s, n_y, n_d, index_ref, *refs):
-    a_refs, w_refs = refs[:n_s], refs[n_s:-3]
-    o_ref, a_held, a_whole = refs[-3:]
-    _, part = a_refs[0].shape
+def mix_kernel(places, n_s, n_w, n_y, n_d, arranged, index_ref, *refs):
+    w_refs, refs = refs[:n_w], refs[n_w:]
     depth, wide = w_refs[0].shape[-2:]
-    many = depth // part
-    for s in range(n_s):
-        a_held[index_ref[n_d + 2 * n_s + s]] = a_refs[s][...]
-    for d in range(n_d):
-        for p in range(many):
-            at = d * depth + p * part
-            a_whole[:, at : at + part] = a_held[index_ref[d] * many + p]
-    for i, j in sorted({(i, j) for i, j, _ in places}):
+    if arranged:
+        a_ref, (out_ref, o_held, sem) = refs[0], refs[-3:]
+    else:
+        out_ref, a_ref, o_held, sem, a_held = refs[-5:]
+        part = refs[0].shape[1]
+        many = depth // part
+        for s in range(n_s):
+            a_held[index_ref[n_d + 2 * n_s + s]] = refs[s][...]
+        for d in range(n_d):
+            for p in range(many):
+                at = d * depth + p * part
+                a_ref[:, at : at + part] = a_held[index_ref[d] * many + p]
+    copies = []
+    for n, (i, j) in enumerate(sorted({(i, j) for i, j, _ in places})):
         total = None
         for d in range(n_d):
             t, plane = places[i, j, d]
-            lhs = a_whole[:, d * depth : (d + 1) * depth]
+            lhs = a_ref[:, d * depth : (d + 1) * depth]
             term = jnp.dot(lhs, w_refs[t][plane], preferred_element_type=jnp.float32)
             total = term if total is None else total + term
+        o_held[n] = total.astype(jnp.bfloat16)
         at = pl.multiple_of(index_ref[n_d + i * n_y + j] * wide, wide)
-        o_ref[:, pl.ds(at, wide)] = total.astype(jnp.bfloat16)
-
-
-def mix(heads, pieces, places, index, n_y, n_d):
-    n_s = len(heads)
+        copies.append(pltpu.make_async_copy(o_held.at[n], out_ref.at[:, pl.ds(at, wide)], sem.at[n]))
+        copies[-1].start()
+    for copy in copies:
+        copy.wait()
+
+
+def mix(heads, pieces, places, index, n_s, n_y, n_d, so_far):
+    arranged = so_far is not None
     rows, part = heads[0].shape
+    part = part // n_s if arranged else part
     wide = pieces[0].shape[2]
+    n_w, n_cols = len(pieces), len(places) // n_d
     vmem = pl.BlockSpec(memory_space=pltpu.VMEM)
+    args = [index, *pieces, *heads]
+    in_specs = [pl.BlockSpec(memory_space=pltpu.SMEM)] + [vmem] * (len(args) - 1)
+    out_shape = [jax.ShapeDtypeStruct((rows, n_s * wide), jnp.bfloat16)]
+    scratch = [pltpu.VMEM((n_cols, rows, wide), jnp.bfloat16), pltpu.SemaphoreType.DMA((n_cols,))]
+    aliases = {}
+    if arranged:
+        aliases = {len(args): 0}
+        args.append(so_far)
+        in_specs.append(ANY)
+    else:
+        out_shape.append(jax.ShapeDtypeStruct((rows, n_s * part), jnp.bfloat16))
+        scratch.append(pltpu.VMEM((n_s, rows, part), jnp.bfloat16))
     return pl.pallas_call(
-        functools.partial(mix_kernel, places, n_s, n_y, n_d),
-        out_shape=jax.ShapeDtypeStruct((rows, n_s * wide), jnp.bfloat16),
-        in_specs=[pl.BlockSpec(memory_space=pltpu.SMEM)] + [vmem] * (n_s + len(pieces)),
-        out_specs=vmem,
-        scratch_shapes=[
-            pltpu.VMEM((n_s, rows, part), jnp.bfloat16),
-            pltpu.VMEM((rows, n_s * part), jnp.bfloat16),
-        ],
+        functools.partial(mix_kernel, places, n_s, n_w, n_y, n_d, arranged),
+        out_shape=out_shape,
+        in_specs=in_specs,
+        out_specs=[ANY] + [vmem] * (len(out_shape) - 1),
+        input_output_aliases=aliases,
+        scratch_shapes=scratch,
         cost_estimate=pl.CostEstimate(
-            flops=2 * rows * n_s * part * n_s * wide,
-            bytes_accessed=2 * n_s * part * n_s * wide,
+            flops=2 * rows * n_s * part * n_cols * wide,
+            bytes_accessed=2 * n_s * part * n_cols * wide,
             transcendentals=0,
         ),
         compiler_params=params(16),
         name="mix",
-    )(index, *heads, *pieces)
+    )(*args)
 
 
 def layout(n_sp, n_dp):
@@ -343,14 +374,22 @@
     up_x, up_c = shift(n_x, n_c, True), shift(n_x, n_c, False)
 
     cut = rows // 2
-    blocks = {(0, 0): [own_rows[:cut], lax.optimization_barrier(own_rows)[cut:]]}
-    for turn in range(1, last + 1):
-        for half in range(2):
-            for i, j in [s for s in s_slots if sum(s) == turn]:
-                before, pairs = ((i, j - 1), up_y) if j else ((i - 1, j), up_z)
-                blocks.setdefault((i, j), [None, None])[half] = lax.ppermute(
-                    blocks[before][half], "sp", pairs
-                )
+    blocks = {(0, 0): [own_rows]}
+    for j in range(1, n_y):
+        blocks[0, j] = [lax.ppermute(blocks[0, j - 1][0], "sp", up_y)]
+    half0 = lax.optimization_barrier(own_rows)[:cut]
+    half1 = lax.optimization_barrier(own_rows)[cut:]
+    column = [half0, half1]
+    for i in range(1, n_z):
+        column = blocks[i, 0] = [lax.ppermute(b, "sp", up_z) for b in column]
+        for j in range(1, n_y):
+            along = list(blocks[i, j - 1])
+            if (i, j) == (n_z - 1, n_y - 1):
+                along[-1] = along[-1][: cut // 2]
+            blocks[i, j] = [lax.ppermute(b, "sp", up_y) for b in along]
+    if n_y > 1:
+        quarter = blocks[0, n_y - 1][0][rows - (cut - cut // 2) :]
+        blocks[n_z - 1, n_y - 1].append(lax.ppermute(quarter, "sp", send_back(n_z, n_y, 1, 0)))
 
     w_blocks = {(0, 0): jnp.concatenate([w_query, w_key, w_value], axis=1)}
     for i in range(1, n_x):
@@ -396,11 +435,11 @@
     ring = [w_out]
     for _ in range(1, n_z):
         ring.append(lax.ppermute(ring[-1], "sp", up_z))
-    parts = 2 if n_z % 2 == 0 else 1
-    size = n_z // parts
+    first = range((n_z + 1) // 2)
+    parts = [first] + [[i] for i in range(len(first), n_z)]
     pieces, places = [], {}
-    for k in range(parts):
-        column = jnp.stack(ring[k * size : (k + 1) * size])
+    for part in parts:
+        column = jnp.stack([ring[i] for i in part])
         for j in range(n_y):
             if j:
                 column = lax.ppermute(column, "sp", up_y)
@@ -412,10 +451,20 @@
                 for c in range(n_c):
                     if c:
                         piece = lax.ppermute(piece, "dp", up_c)
-                    for p in range(size):
-                        places[k * size + p, j, d_slots.index((i, c))] = len(pieces), p
+                    for p, z_slot in enumerate(part):
+                        places[z_slot, j, d_slots.index((i, c))] = len(pieces), p
                     pieces.append(piece)
-    return mix(heads, pieces, places, index, n_y, n_d)[None]
+    out = None
+    group_of = lambda i, j: 0 if j < n_y - 1 else 1 if i < n_z - 1 else 2
+    for n in range(3):
+        mine = {place: at for place, at in places.items() if group_of(*place[:2]) == n}
+        if not mine:
+            continue
+        used = sorted({t for t, _ in mine.values()})
+        mine = {place: (used.index(t), p) for place, (t, p) in mine.items()}
+        out, *arranged = mix(heads, [pieces[t] for t in used], mine, index, n_sp, n_y, n_d, out)
+        heads = arranged or heads
+    return out[None]
 
 
 def solution(mesh):

time: 177 us -> 191 us (1.079)
  waiting for transfers between devices: 72.7 us -> 92 us
  local copies, waits for them, and re-layouts: 6.22 us -> 10.2 us
  Pallas kernels: 44 us -> 40.2 us
  other arithmetic: 9.26 us -> 5.69 us
  starting transfers between devices: 44.3 us -> 41.9 us
    ppermute x3, waiting for transfers between devices: 6.07 us -> 24.4 us  [on_device(): ring.append(lax.ppermute(ring[-1], 'sp', up_z))]
    ppermute x7, starting transfers between devices: 16 us -> 8.77 us  [on_device(): block = lax.ppermute(block, 'sp', send_back(n_z, n_y, i, j))]
    pallas_call x7, Pallas kernels: 24.5 us -> 18.2 us  [attend(): pl.pallas_call(functools.partial(attend_kernel, n_q, group, qs, keys, car...]
    ppermute x14, starting transfers between devices: 13 us -> 18.4 us  [the longest x6 7.16 us: on_device(): blocks[i, j] = [lax.ppermute(b, 'sp', up_y) for b in along]]
    ppermute x4 -> x6, waiting for transfers between devices: 0.03 us -> 4.89 us  [on_device(): row = lax.ppermute(row, 'dp', up_x)]
    ppermute x14, waiting for transfers between devices: 49.3 us -> 44.9 us  [the longest x6 31.3 us: on_device(): blocks[i, j] = [lax.ppermute(b, 'sp', up_y) for b in along]]
    unnamed x16 -> x28, local copies, waits for them, and re-layouts: 1.94 us -> 5.85 us
    ppermute x7, waiting for transfers between devices: 11.9 us -> 15.7 us  [on_device(): block = lax.ppermute(block, 'sp', send_back(n_z, n_y, i, j))]
  transfers between devices with their start and end apart: 41 -> 48, of which waited for: 17 -> 18; matrix products, arithmetic and copies ran while one was open for 9% -> 5% of each run, Pallas kernels for 22% -> 20%
where the time goes in v2:
time: 191 us
  waiting for transfers between devices  92 us (48%)
  starting transfers between devices  41.9 us (22%)
  Pallas kernels  40.2 us (21%)
  local copies, waits for them, and re-layouts  10.2 us (5%)
  other arithmetic  5.69 us (3%)
    ppermute x6, waiting for transfers between devices, on_device(): blocks[i, j] = [lax.ppermute(b, 'sp', up_y) for b in along]  31.3 us
    ppermute x3, waiting for transfers between devices, on_device(): ring.append(lax.ppermute(ring[-1], 'sp', up_z))  24.4 us
    pallas_call x7, Pallas kernels, attend(): pl.pallas_call(functools.partial(attend_kernel, n_q, group, qs, keys, car...  18.2 us
    ppermute x7, waiting for transfers between devices, on_device(): block = lax.ppermute(block, 'sp', send_back(n_z, n_y, i, j))  15.7 us
    pallas_call x4, Pallas kernels, project(): pl.pallas_call(functools.partial(project_kernel, n_b, n_x, n_q, n_kv, fir...  14 us
    ppermute x6, waiting for transfers between devices, on_device(): column = blocks[i, 0] = [lax.ppermute(b, 'sp', up_z) for b in column]  13.6 us
    ppermute x7, starting transfers between devices, on_device(): block = lax.ppermute(block, 'sp', send_back(n_z, n_y, i, j))  8.77 us
    pallas_call x3, Pallas kernels, mix(): pl.pallas_call(functools.partial(mix_kernel, places, n_s, n_w, n_y, n_d,...  7.23 us
  transfers between devices with their start and end apart: 48, of which 18 were waited for; matrix products, arithmetic and copies ran while one was open for 5% of the time, Pallas kernels for 20%

profile of v2, /device:TPU:0, one launch (start us, length us, event | category | flops | bytes accessed | tf_op | source)
XLA Modules:
  0.0 190.6 jit_solution(4986094784947391115)
XLA Ops:
  2.9 3.0 %collective-permute-start.26 = (bf16[512,512]{1,0:T(8,128)(2,1)S(1)}, bf16[512,512]{1,0:T(8,128)(2,1)S(1)}, u32[]{:S(2)}, u32[]{:S(2)}) collective-permute-start(bf16[512,512]{1,0:T(8,128)(2,1)S(1)} %constant_dynamic-update-slice_fusion.refs_0_), channel_id=1, source_target_pairs={{0,2},{1,3},{2,0},{3,1},{4,6},{5,7},{6,4},{7,5},{8,10},{9,11},{10,... | collective-permute-start | bytes 1572872 | tf_op jit(solution)/shard_map/ppermute | solution.py:396
  11.1 5.9 %collective-permute-done = bf16[512,256]{1,0:T(8,128)(2,1)S(1)} collective-permute-done((bf16[512,256]{1,0:T(8,128)(2,1)}, bf16[512,256]{1,0:T(8,128)(2,1)S(1)}, u32[]{:S(2)}, u32[]{:S(2)}) %collective-permute-start) | collective-permute-done | bytes 262176 | tf_op jit(solution)/shard_map/ppermute | solution.py:437
  20.2 13.7 %collective-permute-done.1 = bf16[512,256]{1,0:T(8,128)(2,1)S(1)} collective-permute-done((bf16[512,256]{1,0:T(8,128)(2,1)S(1)}, bf16[512,256]{1,0:T(8,128)(2,1)S(1)}, u32[]{:S(2)}, u32[]{:S(2)}) %collective-permute-start.1) | collective-permute-done | bytes 262176 | tf_op jit(solution)/shard_map/ppermute | solution.py:437
  36.0 9.3 %collective-permute-done.20.refs_3_ = bf16[128,2048]{1,0:T(8,128)(2,1)} collective-permute-done((bf16[128,2048]{1,0:T(8,128)(2,1)}, bf16[128,2048]{1,0:T(8,128)(2,1)}, u32[]{:S(2)}, u32[]{:S(2)}) %collective-permute-start.20) | collective-permute-done | bytes 524320 | tf_op jit(solution)/shard_map/ppermute | solution.py:384
  45.6 4.8 %collective-permute-done.2 = bf16[512,256]{1,0:T(8,128)(2,1)S(1)} collective-permute-done((bf16[512,256]{1,0:T(8,128)(2,1)S(1)}, bf16[512,256]{1,0:T(8,128)(2,1)S(1)}, u32[]{:S(2)}, u32[]{:S(2)}) %collective-permute-start.2) | collective-permute-done | bytes 262176 | tf_op jit(solution)/shard_map/ppermute | solution.py:437
  51.7 4.1 %sine_multiply_fusion = (f32[2048,128]{1,0:T(8,128)S(1)}, f32[2048,128]{1,0:T(8,128)S(1)}) fusion(f32[128]{0:T(128)S(1)} %compare_select_fusion, f32[2048,64]{1,0:T(8,128)S(1)} %get-tuple-element.72, f32[2048,64]{1,0:T(8,128)S(1)} %get-tuple-element.71), kind=kLoop, calls=%fused_computation.1 | loop fusion | flops 524288 | bytes 3146240 | tf_op jit(solution)/shard_map/mul | solution.py:30
  64.8 5.6 %project.4 = (bf16[8,256,256]{2,1,0:T(8,128)(2,1)S(1)}, bf16[8,256,128]{2,1,0:T(8,128)(2,1)S(1)}, bf16[8,256,128]{2,1,0:T(8,128)(2,1)S(1)}) custom-call(s32[28]{0:T(128)S(1)} %stack.97.index_ref, bf16[256,2048]{1,0:T(8,128)(2,1)} %bitcast.21.refs_0_, bf16[256,2048]{1,0:T(8,128)(2,1)} %collective-permute-done.24.refs_1_, ...), custom_call_target="tpu_custom_call" | custom-call | flops 3221225472 | bytes 6029312 | tf_op jit(solution)/shard_map/project/pallas_call | solution.py:165
  72.1 2.7 %attend.7 = (f32[8,256,512]{2,1,0:T(8,128)S(1)}, f32[8,256,256]{2,1,0:T(8,128)S(1)}) custom-call(bf16[8,256,256]{2,1,0:T(8,128)(2,1)S(1)} %get-tuple-element.36.refs_10_.q_ref, bf16[8,256,128]{2,1,0:T(8,128)(2,1)S(1)} %get-tuple-element.37.refs_11_.k_ref, bf16[8,256,128]{2,1,0:T(8,128)(2,1)S(1)} %get-tuple-element.38.refs_12_.v_ref), custom_call_target="tpu_custom_call" | custom-call | flops 2415919104 | bytes 1179648 | tf_op jit(solution)/shard_map/attend/pallas_call | solution.py:259
  75.4 4.3 %collective-permute-done.17.refs_2_ = bf16[128,2048]{1,0:T(8,128)(2,1)S(1)} collective-permute-done((bf16[128,2048]{1,0:T(8,128)(2,1)}, bf16[128,2048]{1,0:T(8,128)(2,1)S(1)}, u32[]{:S(2)}, u32[]{:S(2)}) %collective-permute-start.17) | collective-permute-done | bytes 524320 | tf_op jit(solution)/shard_map/ppermute | solution.py:384
  81.9 9.7 %collective-permute-done.32.refs_1_ = bf16[128,2048]{1,0:T(8,128)(2,1)S(1)} collective-permute-done((bf16[128,2048]{1,0:T(8,128)(2,1)}, bf16[128,2048]{1,0:T(8,128)(2,1)S(1)}, u32[]{:S(2)}, u32[]{:S(2)}) %collective-permute-start.32) | collective-permute-done | bytes 524320 | tf_op jit(solution)/shard_map/ppermute | solution.py:389
  93.1 3.1 %project.5 = (bf16[8,256,256]{2,1,0:T(8,128)(2,1)S(1)}, bf16[8,256,128]{2,1,0:T(8,128)(2,1)S(1)}, bf16[8,256,128]{2,1,0:T(8,128)(2,1)S(1)}) custom-call(s32[28]{0:T(128)S(1)} %stack.97.index_ref, bf16[128,2048]{1,0:T(8,128)(2,1)S(1)} %collective-permute-done.31.refs_0_, ...), custom_call_target="tpu_custom_call", output_to_operand_aliasing={{0}: (11, {}), {1}: (12, {}), {2}: (13, {})} | custom-call | flops 2147483648 | bytes 4718592 | tf_op jit(solution)/shard_map/project/pallas_call | solution.py:165
  99.1 2.7 %attend.9 = (f32[8,256,512]{2,1,0:T(8,128)S(1)}, f32[8,256,256]{2,1,0:T(8,128)S(1)}) custom-call(bf16[8,256,256]{2,1,0:T(8,128)(2,1)S(1)} %get-tuple-element.39.refs_10_.q_ref, bf16[8,256,128]{2,1,0:T(8,128)(2,1)S(1)} %get-tuple-element.40.refs_11_.k_ref, ...), custom_call_target="tpu_custom_call", output_to_operand_aliasing={{0}: (3, {}), {1}: (4, {})} | custom-call | flops 2684354560 | bytes 786432 | tf_op jit(solution)/shard_map/attend/pallas_call | solution.py:259
  103.4 10.7 %collective-permute-done.29.refs_0_ = bf16[128,2048]{1,0:T(8,128)(2,1)S(1)} collective-permute-done((bf16[128,2048]{1,0:T(8,128)(2,1)S(1)}, bf16[128,2048]{1,0:T(8,128)(2,1)S(1)}, u32[]{:S(2)}, u32[]{:S(2)}) %collective-permute-start.29) | collective-permute-done | bytes 524320 | tf_op jit(solution)/shard_map/ppermute | solution.py:389
  114.1 3.8 %collective-permute-start.25 = (bf16[64,2048]{1,0:T(8,128)(2,1)S(1)}, bf16[64,2048]{1,0:T(8,128)(2,1)S(1)}, u32[]{:S(2)}, u32[]{:S(2)}) collective-permute-start(bf16[64,2048]{1,0:T(8,128)(2,1)S(1)} %slice.19), channel_id=1, source_target_pairs={{0,24},{4,28},{8,0},{12,4},{16,8},{20,12},{24,16},{28,20},{1,25},{... | collective-permute-start | bytes 786440 | tf_op jit(solution)/shard_map/ppermute | solution.py:392
  117.9 6.5 %collective-permute-done.30.refs_1_ = bf16[128,2048]{1,0:T(8,128)(2,1)S(1)} collective-permute-done((bf16[128,2048]{1,0:T(8,128)(2,1)}, bf16[128,2048]{1,0:T(8,128)(2,1)S(1)}, u32[]{:S(2)}, u32[]{:S(2)}) %collective-permute-start.30) | collective-permute-done | bytes 524320 | tf_op jit(solution)/shard_map/ppermute | solution.py:389
  126.0 3.2 %project.6 = (bf16[8,256,256]{2,1,0:T(8,128)(2,1)S(1)}, bf16[8,256,128]{2,1,0:T(8,128)(2,1)S(1)}, bf16[8,256,128]{2,1,0:T(8,128)(2,1)S(1)}) custom-call(s32[28]{0:T(128)S(1)} %stack.97.index_ref, bf16[128,2048]{1,0:T(8,128)(2,1)S(1)} %collective-permute-done.29.refs_0_, ...), custom_call_target="tpu_custom_call", output_to_operand_aliasing={{0}: (11, {}), {1}: (12, {}), {2}: (13, {})} | custom-call | flops 2147483648 | bytes 4718592 | tf_op jit(solution)/shard_map/project/pallas_call | solution.py:165
  129.7 3.5 %attend.10 = (f32[8,256,512]{2,1,0:T(8,128)S(1)}, f32[8,256,256]{2,1,0:T(8,128)S(1)}) custom-call(bf16[8,256,256]{2,1,0:T(8,128)(2,1)S(1)} %get-tuple-element.42.refs_7_.q_ref, bf16[8,256,128]{2,1,0:T(8,128)(2,1)S(1)} %get-tuple-element.43.refs_8_.k_ref, ...), custom_call_target="tpu_custom_call", output_to_operand_aliasing={{0}: (3, {}), {1}: (4, {})} | custom-call | flops 2684354560 | bytes 1966080 | tf_op jit(solution)/shard_map/attend/pallas_call | solution.py:259
  137.0 3.6 %attend.11 = (f32[8,256,512]{2,1,0:T(8,128)S(1)}, f32[8,256,256]{2,1,0:T(8,128)S(1)}) custom-call(bf16[8,256,256]{2,1,0:T(8,128)(2,1)S(1)} %get-tuple-element.42.refs_7_.q_ref, bf16[8,256,128]{2,1,0:T(8,128)(2,1)S(1)} %get-tuple-element.43.refs_8_.k_ref, ...), custom_call_target="tpu_custom_call", output_to_operand_aliasing={{0}: (3, {}), {1}: (4, {})} | custom-call | flops 3758096384 | bytes 786432 | tf_op jit(solution)/shard_map/attend/pallas_call | solution.py:259
  140.5 3.7 %collective-permute-done.19.refs_0_ = bf16[128,2048]{1,0:T(8,128)(2,1)S(1)} collective-permute-done((bf16[128,2048]{1,0:T(8,128)(2,1)S(1)}, bf16[128,2048]{1,0:T(8,128)(2,1)S(1)}, u32[]{:S(2)}, u32[]{:S(2)}) %collective-permute-start.19) | collective-permute-done | bytes 524320 | tf_op jit(solution)/shard_map/ppermute | solution.py:389
  155.7 4.7 %collective-permute-done.5.refs_2_ = bf16[1,512,256]{2,1,0:T(8,128)(2,1)S(1)} collective-permute-done((bf16[1,512,256]{2,1,0:T(8,128)(2,1)S(1)}, bf16[1,512,256]{2,1,0:T(8,128)(2,1)S(1)}, u32[]{:S(2)}, u32[]{:S(2)}) %collective-permute-start.5) | collective-permute-done | bytes 262176 | tf_op jit(solution)/shard_map/ppermute | solution.py:449
  160.4 3.5 %collective-permute-start.34 = (bf16[256,256]{1,0:T(8,128)(2,1)S(1)}, bf16[256,256]{1,0:T(8,128)(2,1)S(1)}, u32[]{:S(2)}, u32[]{:S(2)}) collective-permute-start(bf16[256,256]{1,0:T(8,128)(2,1)S(1)} %get-tuple-element.60), channel_id=1, source_target_pairs={{0,24},{4,28},{8,0},{12,4},{16,8},{20,12},{24,16},{28,20},{1,25},{... | collective-permute-start | bytes 393224 | tf_op jit(solution)/shard_map/ppermute | solution.py:432
  164.1 3.8 %collective-permute-done.34.refs_14_ = bf16[256,256]{1,0:T(8,128)(2,1)S(1)} collective-permute-done((bf16[256,256]{1,0:T(8,128)(2,1)S(1)}, bf16[256,256]{1,0:T(8,128)(2,1)S(1)}, u32[]{:S(2)}, u32[]{:S(2)}) %collective-permute-start.34) | collective-permute-done | bytes 131104 | tf_op jit(solution)/shard_map/ppermute | solution.py:432
  172.7 8.5 %collective-permute-done.36.refs_16_ = bf16[256,256]{1,0:T(8,128)(2,1)S(1)} collective-permute-done((bf16[256,256]{1,0:T(8,128)(2,1)S(1)}, bf16[256,256]{1,0:T(8,128)(2,1)S(1)}, u32[]{:S(2)}, u32[]{:S(2)}) %collective-permute-start.36) | collective-permute-done | bytes 131104 | tf_op jit(solution)/shard_map/ppermute | solution.py:432
  183.2 3.3 %mix.3 = (bf16[256,2048]{1,0:T(8,128)(2,1)}, bf16[256,2048]{1,0:T(8,128)(2,1)S(1)}) custom-call(s32[28]{0:T(128)S(1)} %stack.97.index_ref, bf16[2,512,256]{2,1,0:T(8,128)(2,1)S(1)} %pad_maximum_fusion.1.refs_0_, bf16[2,512,256]{2,1,0:T(8,128)(2,1)} %collective-permute-done.7.refs_1_, bf16[2,512,256]{2,1,0:T(8,128)(2,1)} %collective-permute-done.8.refs_2_, ...), custom_call_target="tpu_custom_call" | custom-call | flops 1073741824 | bytes 4194304 | tf_op jit(solution)/shard_map/mix/pallas_call | solution.py:325
  (128 shorter events, 61.9 us)
Async XLA Ops:
  5.9 28.4 %collective-permute-start.27 = (bf16[512,512]{1,0:T(8,128)(2,1)S(1)}, bf16[512,512]{1,0:T(8,128)(2,1)S(1)}, u32[]{:S(2)}, u32[]{:S(2)}) collective-permute-start(bf16[512,512]{1,0:T(8,128)(2,1)S(1)} %constant_dynamic-update-slice_fusion.refs_0_), channel_id=1, source_target_pairs={{0,1},{1,0},{2,3},{3,2},{4,5},{5,4},{6,7},{7,6},{8,9},{9,8},{10,11... | collective-permute-start | bytes 1572872 | tf_op jit(solution)/shard_map/ppermute | solution.py:399
  9.6 24.7 %collective-permute-start.16 = (bf16[128,2048]{1,0:T(8,128)(2,1)S(1)}, bf16[128,2048]{1,0:T(8,128)(2,1)}, u32[]{:S(2)}, u32[]{:S(2)}) collective-permute-start(bf16[128,2048]{1,0:T(8,128)(2,1)S(1)} %get-tuple-element.70), channel_id=1, source_target_pairs={{0,8},{4,12},{8,16},{12,20},{16,24},{20,28},{24,0},{28,4},{1,9},{5... | collective-permute-start | bytes 1572872 | tf_op jit(solution)/shard_map/ppermute | solution.py:384
  17.1 16.9 %collective-permute-start.1 = (bf16[512,256]{1,0:T(8,128)(2,1)S(1)}, bf16[512,256]{1,0:T(8,128)(2,1)S(1)}, u32[]{:S(2)}, u32[]{:S(2)}) collective-permute-start(bf16[512,256]{1,0:T(8,128)(2,1)S(1)} %collective-permute-done), channel_id=1, source_target_pairs={{0,8},{4,12},{8,16},{12,20},{16,24},{20,28},{24,0},{28,4},{1,9},{5... | collective-permute-start | bytes 786440 | tf_op jit(solution)/shard_map/ppermute | solution.py:437
  17.1 46.2 %collective-permute-start.24 = (bf16[256,2048]{1,0:T(8,128)(2,1)}, bf16[256,2048]{1,0:T(8,128)(2,1)}, u32[]{:S(2)}, u32[]{:S(2)}) collective-permute-start(bf16[256,2048]{1,0:T(8,128)(2,1)} %bitcast.21.refs_0_), channel_id=1, source_target_pairs={{0,4},{4,0},{8,12},{12,8},{16,20},{20,16},{24,28},{28,24},{1,5},{5... | collective-permute-start | bytes 3145736 | tf_op jit(solution)/shard_map/ppermute | solution.py:379
  18.8 26.4 %collective-permute-start.20 = (bf16[128,2048]{1,0:T(8,128)(2,1)}, bf16[128,2048]{1,0:T(8,128)(2,1)}, u32[]{:S(2)}, u32[]{:S(2)}) collective-permute-start(bf16[128,2048]{1,0:T(8,128)(2,1)} %get-tuple-element.69), channel_id=1, source_target_pairs={{0,8},{4,12},{8,16},{12,20},{16,24},{20,28},{24,0},{28,4},{1,9},{5... | collective-permute-start | bytes 1572872 | tf_op jit(solution)/shard_map/ppermute | solution.py:384
  34.3 16.6 %collective-permute-start.28 = (bf16[512,512]{1,0:T(8,128)(2,1)S(1)}, bf16[512,512]{1,0:T(8,128)(2,1)S(1)}, u32[]{:S(2)}, u32[]{:S(2)}) collective-permute-start(bf16[512,512]{1,0:T(8,128)(2,1)S(1)} %collective-permute-done.26.refs_1_), channel_id=1, source_target_pairs={{0,1},{1,0},{2,3},{3,2},{4,5},{5,4},{6,7},{7,6},{8,9},{9,8},{10,11... | collective-permute-start | bytes 1572872 | tf_op jit(solution)/shard_map/ppermute | solution.py:399
  51.7 18.8 %collective-permute-start.21 = (bf16[128,2048]{1,0:T(8,128)(2,1)}, bf16[128,2048]{1,0:T(8,128)(2,1)}, u32[]{:S(2)}, u32[]{:S(2)}) collective-permute-start(bf16[128,2048]{1,0:T(8,128)(2,1)} %collective-permute-done.20.refs_3_), channel_id=1, source_target_pairs={{0,8},{4,12},{8,16},{12,20},{16,24},{20,28},{24,0},{28,4},{1,9},{5... | collective-permute-start | bytes 1572872 | tf_op jit(solution)/shard_map/ppermute | solution.py:384
  61.5 18.2 %collective-permute-start.17 = (bf16[128,2048]{1,0:T(8,128)(2,1)}, bf16[128,2048]{1,0:T(8,128)(2,1)S(1)}, u32[]{:S(2)}, u32[]{:S(2)}) collective-permute-start(bf16[128,2048]{1,0:T(8,128)(2,1)} %collective-permute-done.16.refs_2_), channel_id=1, source_target_pairs={{0,8},{4,12},{8,16},{12,20},{16,24},{20,28},{24,0},{28,4},{1,9},{5... | collective-permute-start | bytes 1572872 | tf_op jit(solution)/shard_map/ppermute | solution.py:384
  62.8 17.6 %collective-permute-start.31 = (bf16[128,2048]{1,0:T(8,128)(2,1)}, bf16[128,2048]{1,0:T(8,128)(2,1)S(1)}, u32[]{:S(2)}, u32[]{:S(2)}) collective-permute-start(bf16[128,2048]{1,0:T(8,128)(2,1)} %collective-permute-done.16.refs_2_), channel_id=1, source_target_pairs={{0,4},{4,0},{8,12},{12,8},{16,20},{20,16},{24,28},{28,24},{1,5},{5... | collective-permute-start | bytes 1572872 | tf_op jit(solution)/shard_map/ppermute | solution.py:389
  63.3 28.3 %collective-permute-start.32 = (bf16[128,2048]{1,0:T(8,128)(2,1)}, bf16[128,2048]{1,0:T(8,128)(2,1)S(1)}, u32[]{:S(2)}, u32[]{:S(2)}) collective-permute-start(bf16[128,2048]{1,0:T(8,128)(2,1)} %collective-permute-done.20.refs_3_), channel_id=1, source_target_pairs={{0,4},{4,0},{8,12},{12,8},{16,20},{20,16},{24,28},{28,24},{1,5},{5... | collective-permute-start | bytes 1572872 | tf_op jit(solution)/shard_map/ppermute | solution.py:389
  70.5 28.0 %collective-permute-start.22 = (bf16[128,2048]{1,0:T(8,128)(2,1)}, bf16[128,2048]{1,0:T(8,128)(2,1)S(1)}, u32[]{:S(2)}, u32[]{:S(2)}) collective-permute-start(bf16[128,2048]{1,0:T(8,128)(2,1)} %collective-permute-done.21.refs_3_), channel_id=1, source_target_pairs={{0,8},{4,12},{8,16},{12,20},{16,24},{20,28},{24,0},{28,4},{1,9},{5... | collective-permute-start | bytes 1572872 | tf_op jit(solution)/shard_map/ppermute | solution.py:384
  74.8 28.0 %collective-permute-start.40 = (bf16[2,512,256]{2,1,0:T(8,128)(2,1)S(1)}, bf16[2,512,256]{2,1,0:T(8,128)(2,1)S(1)}, u32[]{:S(2)}, u32[]{:S(2)}) collective-permute-start(bf16[2,512,256]{2,1,0:T(8,128)(2,1)S(1)} %pad_maximum_fusion.1.refs_0_), channel_id=1, source_target_pairs={{0,4},{4,0},{8,12},{12,8},{16,20},{20,16},{24,28},{28,24},{1,5},{5... | collective-permute-start | bytes 1572872 | tf_op jit(solution)/shard_map/ppermute | solution.py:445
  79.7 23.1 %collective-permute-start.18 = (bf16[128,2048]{1,0:T(8,128)(2,1)S(1)}, bf16[128,2048]{1,0:T(8,128)(2,1)S(1)}, u32[]{:S(2)}, u32[]{:S(2)}) collective-permute-start(bf16[128,2048]{1,0:T(8,128)(2,1)S(1)} %collective-permute-done.17.refs_2_), channel_id=1, source_target_pairs={{0,8},{4,12},{8,16},{12,20},{16,24},{20,28},{24,0},{28,4},{1,9},{5... | collective-permute-start | bytes 1572872 | tf_op jit(solution)/shard_map/ppermute | solution.py:384
  80.4 33.7 %collective-permute-start.29 = (bf16[128,2048]{1,0:T(8,128)(2,1)S(1)}, bf16[128,2048]{1,0:T(8,128)(2,1)S(1)}, u32[]{:S(2)}, u32[]{:S(2)}) collective-permute-start(bf16[128,2048]{1,0:T(8,128)(2,1)S(1)} %collective-permute-done.17.refs_2_), channel_id=1, source_target_pairs={{0,4},{4,0},{8,12},{12,8},{16,20},{20,16},{24,28},{28,24},{1,5},{5... | collective-permute-start | bytes 1572872 | tf_op jit(solution)/shard_map/ppermute | solution.py:389
  91.6 32.8 %collective-permute-start.30 = (bf16[128,2048]{1,0:T(8,128)(2,1)}, bf16[128,2048]{1,0:T(8,128)(2,1)S(1)}, u32[]{:S(2)}, u32[]{:S(2)}) collective-permute-start(bf16[128,2048]{1,0:T(8,128)(2,1)} %collective-permute-done.21.refs_3_), channel_id=1, source_target_pairs={{0,4},{4,0},{8,12},{12,8},{16,20},{20,16},{24,28},{28,24},{1,5},{5... | collective-permute-start | bytes 1572872 | tf_op jit(solution)/shard_map/ppermute | solution.py:389
  98.4 30.7 %collective-permute-start.14 = (bf16[1,512,256]{2,1,0:T(8,128)(2,1)S(1)}, bf16[1,512,256]{2,1,0:T(8,128)(2,1)S(1)}, u32[]{:S(2)}, u32[]{:S(2)}) collective-permute-start(bf16[1,512,256]{2,1,0:T(8,128)(2,1)S(1)} %bitcast.27), channel_id=1, source_target_pairs={{0,2},{1,3},{2,0},{3,1},{4,6},{5,7},{6,4},{7,5},{8,10},{9,11},{10,... | collective-permute-start | bytes 786440 | tf_op jit(solution)/shard_map/ppermute | solution.py:449
  102.9 32.0 %collective-permute-start.13 = (bf16[1,512,256]{2,1,0:T(8,128)(2,1)S(1)}, bf16[1,512,256]{2,1,0:T(8,128)(2,1)S(1)}, u32[]{:S(2)}, u32[]{:S(2)}) collective-permute-start(bf16[1,512,256]{2,1,0:T(8,128)(2,1)S(1)} %bitcast.28), channel_id=1, source_target_pairs={{0,1},{1,0},{2,3},{3,2},{4,5},{5,4},{6,7},{7,6},{8,9},{9,8},{10,11... | collective-permute-start | bytes 786440 | tf_op jit(solution)/shard_map/ppermute | solution.py:453
  102.9 30.4 %collective-permute-start.12 = (bf16[1,512,256]{2,1,0:T(8,128)(2,1)S(1)}, bf16[1,512,256]{2,1,0:T(8,128)(2,1)S(1)}, u32[]{:S(2)}, u32[]{:S(2)}) collective-permute-start(bf16[1,512,256]{2,1,0:T(8,128)(2,1)S(1)} %copy-done.7), channel_id=1, source_target_pairs={{0,1},{1,0},{2,3},{3,2},{4,5},{5,4},{6,7},{7,6},{8,9},{9,8},{10,11... | collective-permute-start | bytes 786440 | tf_op jit(solution)/shard_map/ppermute | solution.py:453
  114.1 20.8 %collective-permute-start.25 = (bf16[64,2048]{1,0:T(8,128)(2,1)S(1)}, bf16[64,2048]{1,0:T(8,128)(2,1)S(1)}, u32[]{:S(2)}, u32[]{:S(2)}) collective-permute-start(bf16[64,2048]{1,0:T(8,128)(2,1)S(1)} %slice.19), channel_id=1, source_target_pairs={{0,24},{4,28},{8,0},{12,4},{16,8},{20,12},{24,16},{28,20},{1,25},{... | collective-permute-start | bytes 786440 | tf_op jit(solution)/shard_map/ppermute | solution.py:392
  134.9 20.3 %collective-permute-start.9 = (bf16[2,512,256]{2,1,0:T(8,128)(2,1)}, bf16[2,512,256]{2,1,0:T(8,128)(2,1)S(1)}, u32[]{:S(2)}, u32[]{:S(2)}) collective-permute-start(bf16[2,512,256]{2,1,0:T(8,128)(2,1)} %collective-permute-done.8.refs_2_), channel_id=1, source_target_pairs={{0,1},{1,0},{2,3},{3,2},{4,5},{5,4},{6,7},{7,6},{8,9},{9,8},{10,11... | collective-permute-start | bytes 1572872 | tf_op jit(solution)/shard_map/ppermute | solution.py:453
  135.5 19.9 %collective-permute-start.42 = (bf16[2,512,256]{2,1,0:T(8,128)(2,1)S(1)}, bf16[2,512,256]{2,1,0:T(8,128)(2,1)S(1)}, u32[]{:S(2)}, u32[]{:S(2)}) collective-permute-start(bf16[2,512,256]{2,1,0:T(8,128)(2,1)S(1)} %collective-permute-done.40.refs_0_), channel_id=1, source_target_pairs={{0,2},{1,3},{2,0},{3,1},{4,6},{5,7},{6,4},{7,5},{8,10},{9,11},{10,... | collective-permute-start | bytes 1572872 | tf_op jit(solution)/shard_map/ppermute | solution.py:449
  155.2 31.3 %collective-permute-start.41 = (bf16[2,512,256]{2,1,0:T(8,128)(2,1)S(1)}, bf16[2,512,256]{2,1,0:T(8,128)(2,1)S(1)}, u32[]{:S(2)}, u32[]{:S(2)}) collective-permute-start(bf16[2,512,256]{2,1,0:T(8,128)(2,1)S(1)} %collective-permute-done.40.refs_0_), channel_id=1, source_target_pairs={{0,1},{1,0},{2,3},{3,2},{4,5},{5,4},{6,7},{7,6},{8,9},{9,8},{10,11... | collective-permute-start | bytes 1572872 | tf_op jit(solution)/shard_map/ppermute | solution.py:453
  155.3 31.2 %collective-permute-start.43 = (bf16[2,512,256]{2,1,0:T(8,128)(2,1)S(1)}, bf16[2,512,256]{2,1,0:T(8,128)(2,1)S(1)}, u32[]{:S(2)}, u32[]{:S(2)}) collective-permute-start(bf16[2,512,256]{2,1,0:T(8,128)(2,1)S(1)} %collective-permute-done.42.refs_2_), channel_id=1, source_target_pairs={{0,1},{1,0},{2,3},{3,2},{4,5},{5,4},{6,7},{7,6},{8,9},{9,8},{10,11... | collective-permute-start | bytes 1572872 | tf_op jit(solution)/shard_map/ppermute | solution.py:453
  164.0 17.3 %collective-permute-start.36 = (bf16[256,256]{1,0:T(8,128)(2,1)S(1)}, bf16[256,256]{1,0:T(8,128)(2,1)S(1)}, u32[]{:S(2)}, u32[]{:S(2)}) collective-permute-start(bf16[256,256]{1,0:T(8,128)(2,1)S(1)} %get-tuple-element.62), channel_id=1, source_target_pairs={{0,16},{4,20},{8,24},{12,28},{16,0},{20,4},{24,8},{28,12},{1,17},{... | collective-permute-start | bytes 393224 | tf_op jit(solution)/shard_map/ppermute | solution.py:432
  (37 other events, 359.7 us)

commit v3 on v2

--- a/solution.py
+++ b/solution.py
@@ -362,7 +362,11 @@
     s_slots = [(i, j) for i in range(n_z) for j in range(n_y)]
     n_d = len(d_slots)
     last = n_z + n_y - 2
-    order = sorted(s_slots, key=lambda s: max(sum(s), 1))
+    stages = [[s for s in s_slots if max(sum(s), 1) == turn] for turn in range(1, last + 1)]
+    if last > 2:
+        late = sorted(stages[-2], key=lambda s: s[0])
+        stages[-2:-1] = [late[:-1], late[-1:]]
+    order = sum(stages, [])
     s_owner = {s: owner_of("sp", n_z, n_y, *s) for s in s_slots}
     index = jnp.stack(
         [owner_of("dp", n_x, n_c, *s) for s in d_slots]
@@ -407,14 +411,13 @@
 
     held = state = None
     n_held = n_done = 0
-    for turn in range(1, last + 1):
-        ready = [s for s in order if max(sum(s), 1) == turn]
+    for turn, ready in enumerate(stages, 1):
         held = project(
             [blocks[s] for s in ready], [s_slots.index(s) for s in ready], n_held, weight, index, n_d,
             qk_gain, *tables, n_q, n_kv, held, n_sp,
         )
         n_held += len(ready)
-        old, final = (0, n_done), turn == last
+        old, final = (0, n_done), turn == len(stages)
         fresh = (n_done, n_held)
         carry = functools.partial(attend, n_q=n_q, group=group)
         if n_done:

time: 191 us -> 185 us (0.969)
  waiting for transfers between devices: 92 us -> 83 us
  starting transfers between devices: 41.9 us -> 46.7 us
  local copies, waits for them, and re-layouts: 10.2 us -> 5.48 us
  other arithmetic: 5.69 us -> 8.13 us
    ppermute x7, starting transfers between devices: 8.77 us -> 19.7 us  [on_device(): block = lax.ppermute(block, 'sp', send_back(n_z, n_y, i, j))]
    ppermute x3, waiting for transfers between devices: 24.4 us -> 33.9 us  [on_device(): ring.append(lax.ppermute(ring[-1], 'sp', up_z))]
    ppermute x7, waiting for transfers between devices: 15.7 us -> 6.88 us  [on_device(): block = lax.ppermute(block, 'sp', send_back(n_z, n_y, i, j))]
    ppermute x6, waiting for transfers between devices: 31.3 us -> 25.7 us  [on_device(): blocks[i, j] = [lax.ppermute(b, 'sp', up_y) for b in along]]
    unnamed x28 -> x8, local copies, waits for them, and re-layouts: 5.85 us -> 1.92 us
    ppermute x6, waiting for transfers between devices: 4.89 us -> 1.02 us  [on_device(): row = lax.ppermute(row, 'dp', up_x)]
    ppermute x6, waiting for transfers between devices: 13.6 us -> 10.2 us  [on_device(): column = blocks[i, 0] = [lax.ppermute(b, 'sp', up_z) for b in column]]
    ppermute x6, starting transfers between devices: 3.86 us -> 7.17 us  [on_device(): row = lax.ppermute(row, 'dp', up_x)]
  transfers between devices with their start and end apart: 48 -> 48, of which waited for: 18 -> 17; matrix products, arithmetic and copies ran while one was open for 5% -> 6% of each run, Pallas kernels for 20% -> 21%
where the time goes in v3:
time: 185 us
  waiting for transfers between devices  83 us (45%)
  starting transfers between devices  46.7 us (25%)
  Pallas kernels  40.9 us (22%)
  other arithmetic  8.13 us (4%)
  local copies, waits for them, and re-layouts  5.48 us (3%)
    ppermute x3, waiting for transfers between devices, on_device(): ring.append(lax.ppermute(ring[-1], 'sp', up_z))  33.9 us
    ppermute x6, waiting for transfers between devices, on_device(): blocks[i, j] = [lax.ppermute(b, 'sp', up_y) for b in along]  25.7 us
    pallas_call x9, Pallas kernels, attend(): pl.pallas_call(functools.partial(attend_kernel, n_q, group, qs, keys, car...  19.9 us
    ppermute x7, starting transfers between devices, on_device(): block = lax.ppermute(block, 'sp', send_back(n_z, n_y, i, j))  19.7 us
    pallas_call x5, Pallas kernels, project(): pl.pallas_call(functools.partial(project_kernel, n_b, n_x, n_q, n_kv, fir...  13.8 us
    ppermute x6, waiting for transfers between devices, on_device(): column = blocks[i, 0] = [lax.ppermute(b, 'sp', up_z) for b in column]  10.2 us
    ppermute x6, starting transfers between devices, on_device(): row = lax.ppermute(row, 'dp', up_x)  7.17 us
    ppermute x7, waiting for transfers between devices, on_device(): block = lax.ppermute(block, 'sp', send_back(n_z, n_y, i, j))  6.88 us
  transfers between devices with their start and end apart: 48, of which 17 were waited for; matrix products, arithmetic and copies ran while one was open for 6% of the time, Pallas kernels for 21%

profile of v3, /device:TPU:0, one launch (start us, length us, event | category | flops | bytes accessed | tf_op | source)
XLA Modules:
  0.0 184.9 jit_solution(7045457748377224416)
XLA Ops:
  2.9 3.0 %collective-permute-start.26 = (bf16[512,512]{1,0:T(8,128)(2,1)S(1)}, bf16[512,512]{1,0:T(8,128)(2,1)S(1)}, u32[]{:S(2)}, u32[]{:S(2)}) collective-permute-start(bf16[512,512]{1,0:T(8,128)(2,1)S(1)} %constant_dynamic-update-slice_fusion.refs_0_), channel_id=1, source_target_pairs={{0,2},{1,3},{2,0},{3,1},{4,6},{5,7},{6,4},{7,5},{8,10},{9,11},{10,... | collective-permute-start | bytes 1572872 | tf_op jit(solution)/shard_map/ppermute | solution.py:400
  9.0 2.3 %fusion.10 = (bf16[128,2048]{1,0:T(8,128)(2,1)}, bf16[128,2048]{1,0:T(8,128)(2,1)}) fusion(bf16[256,2048]{1,0:T(8,128)(2,1)} %bitcast.24), kind=kLoop, calls=%fused_computation.25 | loop fusion | bytes 2097152 | tf_op jit(solution)/shard_map/slice | solution.py:385
  13.1 5.6 %collective-permute-done = bf16[512,256]{1,0:T(8,128)(2,1)} collective-permute-done((bf16[512,256]{1,0:T(8,128)(2,1)}, bf16[512,256]{1,0:T(8,128)(2,1)}, u32[]{:S(2)}, u32[]{:S(2)}) %collective-permute-start) | collective-permute-done | bytes 262176 | tf_op jit(solution)/shard_map/ppermute | solution.py:440
  22.2 23.8 %collective-permute-done.1 = bf16[512,256]{1,0:T(8,128)(2,1)S(1)} collective-permute-done((bf16[512,256]{1,0:T(8,128)(2,1)}, bf16[512,256]{1,0:T(8,128)(2,1)S(1)}, u32[]{:S(2)}, u32[]{:S(2)}) %collective-permute-start.1) | collective-permute-done | bytes 262176 | tf_op jit(solution)/shard_map/ppermute | solution.py:440
  47.8 5.1 %sine_multiply_fusion = (f32[2048,128]{1,0:T(8,128)S(1)}, f32[2048,128]{1,0:T(8,128)S(1)}) fusion(f32[128]{0:T(128)S(1)} %compare_select_fusion, f32[2048,64]{1,0:T(8,128)} %get-tuple-element.86, f32[2048,64]{1,0:T(8,128)} %get-tuple-element.85), kind=kLoop, calls=%fused_computation.1 | loop fusion | flops 524288 | bytes 3146240 | tf_op jit(solution)/shard_map/mul | solution.py:30
  53.0 4.5 %collective-permute-done.2 = bf16[512,256]{1,0:T(8,128)(2,1)S(1)} collective-permute-done((bf16[512,256]{1,0:T(8,128)(2,1)S(1)}, bf16[512,256]{1,0:T(8,128)(2,1)S(1)}, u32[]{:S(2)}, u32[]{:S(2)}) %collective-permute-start.2) | collective-permute-done | bytes 262176 | tf_op jit(solution)/shard_map/ppermute | solution.py:440
  63.0 5.8 %collective-permute-done.17.refs_2_ = bf16[128,2048]{1,0:T(8,128)(2,1)S(1)} collective-permute-done((bf16[128,2048]{1,0:T(8,128)(2,1)}, bf16[128,2048]{1,0:T(8,128)(2,1)S(1)}, u32[]{:S(2)}, u32[]{:S(2)}) %collective-permute-start.17) | collective-permute-done | bytes 524320 | tf_op jit(solution)/shard_map/ppermute | solution.py:388
  69.3 4.5 %project.5 = (bf16[8,256,256]{2,1,0:T(8,128)(2,1)S(1)}, bf16[8,256,128]{2,1,0:T(8,128)(2,1)S(1)}, bf16[8,256,128]{2,1,0:T(8,128)(2,1)S(1)}) custom-call(s32[28]{0:T(128)S(1)} %stack.97.index_ref, bf16[256,2048]{1,0:T(8,128)(2,1)S(1)} %bitcast.25, bf16[256,2048]{1,0:T(8,128)(2,1)S(1)} %collective-permute-done.24.refs_1_, ...), custom_call_target="tpu_custom_call" | custom-call | flops 3221225472 | bytes 6029312 | tf_op jit(solution)/shard_map/project/pallas_call | solution.py:165
  73.8 4.4 %collective-permute-done.21.refs_3_ = bf16[128,2048]{1,0:T(8,128)(2,1)S(1)} collective-permute-done((bf16[128,2048]{1,0:T(8,128)(2,1)}, bf16[128,2048]{1,0:T(8,128)(2,1)S(1)}, u32[]{:S(2)}, u32[]{:S(2)}) %collective-permute-start.21) | collective-permute-done | bytes 524320 | tf_op jit(solution)/shard_map/ppermute | solution.py:388
  78.9 4.9 %collective-permute-done.32.refs_1_ = bf16[128,2048]{1,0:T(8,128)(2,1)S(1)} collective-permute-done((bf16[128,2048]{1,0:T(8,128)(2,1)}, bf16[128,2048]{1,0:T(8,128)(2,1)S(1)}, u32[]{:S(2)}, u32[]{:S(2)}) %collective-permute-start.32) | collective-permute-done | bytes 524320 | tf_op jit(solution)/shard_map/ppermute | solution.py:393
  83.8 2.7 %attend.9 = (f32[8,256,512]{2,1,0:T(8,128)S(1)}, f32[8,256,256]{2,1,0:T(8,128)S(1)}) custom-call(bf16[8,256,256]{2,1,0:T(8,128)(2,1)S(1)} %get-tuple-element.43.refs_10_.q_ref, bf16[8,256,128]{2,1,0:T(8,128)(2,1)S(1)} %get-tuple-element.44.refs_11_.k_ref, bf16[8,256,128]{2,1,0:T(8,128)(2,1)S(1)} %get-tuple-element.45.refs_12_.v_ref), custom_call_target="tpu_custom_call" | custom-call | flops 2415919104 | bytes 1179648 | tf_op jit(solution)/shard_map/attend/pallas_call | solution.py:259
  86.5 3.2 %project.6 = (bf16[8,256,256]{2,1,0:T(8,128)(2,1)S(1)}, bf16[8,256,128]{2,1,0:T(8,128)(2,1)S(1)}, bf16[8,256,128]{2,1,0:T(8,128)(2,1)S(1)}) custom-call(s32[28]{0:T(128)S(1)} %stack.97.index_ref, bf16[128,2048]{1,0:T(8,128)(2,1)S(1)} %collective-permute-done.31.refs_0_, ...), custom_call_target="tpu_custom_call", output_to_operand_aliasing={{0}: (11, {}), {1}: (12, {}), {2}: (13, {})} | custom-call | flops 2147483648 | bytes 4718592 | tf_op jit(solution)/shard_map/project/pallas_call | solution.py:165
  90.3 4.7 %collective-permute-done.29.refs_0_ = bf16[128,2048]{1,0:T(8,128)(2,1)S(1)} collective-permute-done((bf16[128,2048]{1,0:T(8,128)(2,1)S(1)}, bf16[128,2048]{1,0:T(8,128)(2,1)S(1)}, u32[]{:S(2)}, u32[]{:S(2)}) %collective-permute-start.29) | collective-permute-done | bytes 524320 | tf_op jit(solution)/shard_map/ppermute | solution.py:393
  97.1 9.1 %collective-permute-done.30.refs_1_ = bf16[128,2048]{1,0:T(8,128)(2,1)S(1)} collective-permute-done((bf16[128,2048]{1,0:T(8,128)(2,1)S(1)}, bf16[128,2048]{1,0:T(8,128)(2,1)S(1)}, u32[]{:S(2)}, u32[]{:S(2)}) %collective-permute-start.30) | collective-permute-done | bytes 524320 | tf_op jit(solution)/shard_map/ppermute | solution.py:393
  108.2 2.7 %attend.11 = (f32[8,256,512]{2,1,0:T(8,128)S(1)}, f32[8,256,256]{2,1,0:T(8,128)S(1)}) custom-call(bf16[8,256,256]{2,1,0:T(8,128)(2,1)S(1)} %get-tuple-element.46.refs_6_.q_ref, bf16[8,256,128]{2,1,0:T(8,128)(2,1)S(1)} %get-tuple-element.47.refs_7_.k_ref, ...), custom_call_target="tpu_custom_call", output_to_operand_aliasing={{0}: (3, {}), {1}: (4, {})} | custom-call | flops 2684354560 | bytes 786432 | tf_op jit(solution)/shard_map/attend/pallas_call | solution.py:259
  113.0 2.5 %attend.12 = (f32[8,256,512]{2,1,0:T(8,128)S(1)}, f32[8,256,256]{2,1,0:T(8,128)S(1)}) custom-call(bf16[8,256,256]{2,1,0:T(8,128)(2,1)S(1)} %get-tuple-element.49.refs_6_.q_ref, bf16[8,256,128]{2,1,0:T(8,128)(2,1)S(1)} %get-tuple-element.50.refs_7_.k_ref, ...), custom_call_target="tpu_custom_call", output_to_operand_aliasing={{0}: (3, {}), {1}: (4, {})} | custom-call | flops 1342177280 | bytes 1966080 | tf_op jit(solution)/shard_map/attend/pallas_call | solution.py:259
  115.6 3.0 %collective-permute-done.44.refs_4_ = bf16[1,512,256]{2,1,0:T(8,128)(2,1)S(1)} collective-permute-done((bf16[1,512,256]{2,1,0:T(8,128)(2,1)S(1)}, bf16[1,512,256]{2,1,0:T(8,128)(2,1)S(1)}, u32[]{:S(2)}, u32[]{:S(2)}) %collective-permute-start.44) | collective-permute-done | bytes 262176 | tf_op jit(solution)/shard_map/ppermute | solution.py:448
  124.8 3.0 %attend.14 = (f32[8,256,512]{2,1,0:T(8,128)S(1)}, f32[8,256,256]{2,1,0:T(8,128)S(1)}) custom-call(bf16[8,256,256]{2,1,0:T(8,128)(2,1)S(1)} %get-tuple-element.52.refs_7_.q_ref, bf16[8,256,128]{2,1,0:T(8,128)(2,1)S(1)} %get-tuple-element.53.refs_8_.k_ref, ...), custom_call_target="tpu_custom_call", output_to_operand_aliasing={{0}: (3, {}), {1}: (4, {})} | custom-call | flops 1610612736 | bytes 2359296 | tf_op jit(solution)/shard_map/attend/pallas_call | solution.py:259
  132.5 7.1 %collective-permute-done.19.refs_0_ = bf16[128,2048]{1,0:T(8,128)(2,1)S(1)} collective-permute-done((bf16[128,2048]{1,0:T(8,128)(2,1)S(1)}, bf16[128,2048]{1,0:T(8,128)(2,1)S(1)}, u32[]{:S(2)}, u32[]{:S(2)}) %collective-permute-start.19) | collective-permute-done | bytes 524320 | tf_op jit(solution)/shard_map/ppermute | solution.py:393
  142.2 2.2 %collective-permute-done.3.refs_0_ = bf16[1,512,256]{2,1,0:T(8,128)(2,1)S(1)} collective-permute-done((bf16[1,512,256]{2,1,0:T(8,128)(2,1)S(1)}, bf16[1,512,256]{2,1,0:T(8,128)(2,1)S(1)}, u32[]{:S(2)}, u32[]{:S(2)}) %collective-permute-start.3) | collective-permute-done | bytes 262176 | tf_op jit(solution)/shard_map/ppermute | solution.py:448
  159.8 2.4 %collective-permute-start.37 = (bf16[256,256]{1,0:T(8,128)(2,1)S(1)}, bf16[256,256]{1,0:T(8,128)(2,1)S(1)}, u32[]{:S(2)}, u32[]{:S(2)}) collective-permute-start(bf16[256,256]{1,0:T(8,128)(2,1)S(1)} %get-tuple-element.77), channel_id=1, source_target_pairs={{0,20},{4,16},{8,28},{12,24},{16,4},{20,0},{24,12},{28,8},{1,21},{... | collective-permute-start | bytes 393224 | tf_op jit(solution)/shard_map/ppermute | solution.py:435
  162.7 11.3 %collective-permute-start.38 = (bf16[256,256]{1,0:T(8,128)(2,1)S(1)}, bf16[256,256]{1,0:T(8,128)(2,1)S(1)}, u32[]{:S(2)}, u32[]{:S(2)}) collective-permute-start(bf16[256,256]{1,0:T(8,128)(2,1)S(1)} %get-tuple-element.78), channel_id=1, source_target_pairs={{0,8},{4,12},{8,16},{12,20},{16,24},{20,28},{24,0},{28,4},{1,9},{5... | collective-permute-start | bytes 393224 | tf_op jit(solution)/shard_map/ppermute | solution.py:435
  178.2 2.6 %mix.3 = (bf16[256,2048]{1,0:T(8,128)(2,1)}, bf16[256,2048]{1,0:T(8,128)(2,1)S(1)}) custom-call(s32[28]{0:T(128)S(1)} %stack.97.index_ref, bf16[2,512,256]{2,1,0:T(8,128)(2,1)S(1)} %pad_maximum_fusion.1.refs_0_, bf16[2,512,256]{2,1,0:T(8,128)(2,1)S(1)} %collective-permute-done.7.refs_1_, bf16[2,512,256]{2,1,0:T(8,128)(2,1)S(1)} %collective-permute-done.8.refs_2_, ...), custom_call_target="tpu_custom_call" | custom-call | flops 1073741824 | bytes 4194304 | tf_op jit(solution)/shard_map/mix/pallas_call | solution.py:325
  180.8 2.3 %mix.4.refs_5_ = bf16[256,2048]{1,0:T(8,128)(2,1)} custom-call(s32[28]{0:T(128)S(1)} %stack.97.index_ref, bf16[2,512,256]{2,1,0:T(8,128)(2,1)S(1)} %collective-permute-done.40.refs_0_, bf16[2,512,256]{2,1,0:T(8,128)(2,1)S(1)} %collective-permute-done.41.refs_1_, ...), custom_call_target="tpu_custom_call", output_to_operand_aliasing={{}: (10, {})} | custom-call | flops 805306368 | bytes 3145728 | tf_op jit(solution)/shard_map/mix/pallas_call | solution.py:325
  (111 shorter events, 61.7 us)
Async XLA Ops:
  5.9 55.5 %collective-permute-start.24 = (bf16[256,2048]{1,0:T(8,128)(2,1)}, bf16[256,2048]{1,0:T(8,128)(2,1)S(1)}, u32[]{:S(2)}, u32[]{:S(2)}) collective-permute-start(bf16[256,2048]{1,0:T(8,128)(2,1)} %bitcast.23), channel_id=1, source_target_pairs={{0,4},{4,0},{8,12},{12,8},{16,20},{20,16},{24,28},{28,24},{1,5},{5... | collective-permute-start | bytes 3145736 | tf_op jit(solution)/shard_map/ppermute | solution.py:383
  11.3 35.3 %collective-permute-start.16 = (bf16[128,2048]{1,0:T(8,128)(2,1)}, bf16[128,2048]{1,0:T(8,128)(2,1)}, u32[]{:S(2)}, u32[]{:S(2)}) collective-permute-start(bf16[128,2048]{1,0:T(8,128)(2,1)} %get-tuple-element.84), channel_id=1, source_target_pairs={{0,8},{4,12},{8,16},{12,20},{16,24},{20,28},{24,0},{28,4},{1,9},{5... | collective-permute-start | bytes 1572872 | tf_op jit(solution)/shard_map/ppermute | solution.py:388
  18.7 27.8 %collective-permute-start.20 = (bf16[128,2048]{1,0:T(8,128)(2,1)}, bf16[128,2048]{1,0:T(8,128)(2,1)}, u32[]{:S(2)}, u32[]{:S(2)}) collective-permute-start(bf16[128,2048]{1,0:T(8,128)(2,1)} %get-tuple-element.83), channel_id=1, source_target_pairs={{0,8},{4,12},{8,16},{12,20},{16,24},{20,28},{24,0},{28,4},{1,9},{5... | collective-permute-start | bytes 1572872 | tf_op jit(solution)/shard_map/ppermute | solution.py:388
  18.7 27.3 %collective-permute-start.1 = (bf16[512,256]{1,0:T(8,128)(2,1)}, bf16[512,256]{1,0:T(8,128)(2,1)S(1)}, u32[]{:S(2)}, u32[]{:S(2)}) collective-permute-start(bf16[512,256]{1,0:T(8,128)(2,1)} %collective-permute-done), channel_id=1, source_target_pairs={{0,8},{4,12},{8,16},{12,20},{16,24},{20,28},{24,0},{28,4},{1,9},{5... | collective-permute-start | bytes 786440 | tf_op jit(solution)/shard_map/ppermute | solution.py:440
  22.0 36.0 %collective-permute-start.28 = (bf16[512,512]{1,0:T(8,128)(2,1)S(1)}, bf16[512,512]{1,0:T(8,128)(2,1)S(1)}, u32[]{:S(2)}, u32[]{:S(2)}) collective-permute-start(bf16[512,512]{1,0:T(8,128)(2,1)S(1)} %collective-permute-done.26.refs_1_), channel_id=1, source_target_pairs={{0,1},{1,0},{2,3},{3,2},{4,5},{5,4},{6,7},{7,6},{8,9},{9,8},{10,11... | collective-permute-start | bytes 1572872 | tf_op jit(solution)/shard_map/ppermute | solution.py:403
  46.6 22.2 %collective-permute-start.17 = (bf16[128,2048]{1,0:T(8,128)(2,1)}, bf16[128,2048]{1,0:T(8,128)(2,1)S(1)}, u32[]{:S(2)}, u32[]{:S(2)}) collective-permute-start(bf16[128,2048]{1,0:T(8,128)(2,1)} %collective-permute-done.16.refs_2_), channel_id=1, source_target_pairs={{0,8},{4,12},{8,16},{12,20},{16,24},{20,28},{24,0},{28,4},{1,9},{5... | collective-permute-start | bytes 1572872 | tf_op jit(solution)/shard_map/ppermute | solution.py:388
  57.5 20.7 %collective-permute-start.31 = (bf16[128,2048]{1,0:T(8,128)(2,1)}, bf16[128,2048]{1,0:T(8,128)(2,1)S(1)}, u32[]{:S(2)}, u32[]{:S(2)}) collective-permute-start(bf16[128,2048]{1,0:T(8,128)(2,1)} %collective-permute-done.16.refs_2_), channel_id=1, source_target_pairs={{0,4},{4,0},{8,12},{12,8},{16,20},{20,16},{24,28},{28,24},{1,5},{5... | collective-permute-start | bytes 1572872 | tf_op jit(solution)/shard_map/ppermute | solution.py:393
  58.0 20.1 %collective-permute-start.21 = (bf16[128,2048]{1,0:T(8,128)(2,1)}, bf16[128,2048]{1,0:T(8,128)(2,1)S(1)}, u32[]{:S(2)}, u32[]{:S(2)}) collective-permute-start(bf16[128,2048]{1,0:T(8,128)(2,1)} %collective-permute-done.20.refs_3_), channel_id=1, source_target_pairs={{0,8},{4,12},{8,16},{12,20},{16,24},{20,28},{24,0},{28,4},{1,9},{5... | collective-permute-start | bytes 1572872 | tf_op jit(solution)/shard_map/ppermute | solution.py:388
  58.0 25.7 %collective-permute-start.32 = (bf16[128,2048]{1,0:T(8,128)(2,1)}, bf16[128,2048]{1,0:T(8,128)(2,1)S(1)}, u32[]{:S(2)}, u32[]{:S(2)}) collective-permute-start(bf16[128,2048]{1,0:T(8,128)(2,1)} %collective-permute-done.20.refs_3_), channel_id=1, source_target_pairs={{0,4},{4,0},{8,12},{12,8},{16,20},{20,16},{24,28},{28,24},{1,5},{5... | collective-permute-start | bytes 1572872 | tf_op jit(solution)/shard_map/ppermute | solution.py:393
  61.4 28.3 %collective-permute-start.8 = (bf16[2,512,256]{2,1,0:T(8,128)(2,1)S(1)}, bf16[2,512,256]{2,1,0:T(8,128)(2,1)S(1)}, u32[]{:S(2)}, u32[]{:S(2)}) collective-permute-start(bf16[2,512,256]{2,1,0:T(8,128)(2,1)S(1)} %pad_maximum_fusion.1.refs_0_), channel_id=1, source_target_pairs={{0,2},{1,3},{2,0},{3,1},{4,6},{5,7},{6,4},{7,5},{8,10},{9,11},{10,... | collective-permute-start | bytes 1572872 | tf_op jit(solution)/shard_map/ppermute | solution.py:452
  68.8 26.2 %collective-permute-start.29 = (bf16[128,2048]{1,0:T(8,128)(2,1)S(1)}, bf16[128,2048]{1,0:T(8,128)(2,1)S(1)}, u32[]{:S(2)}, u32[]{:S(2)}) collective-permute-start(bf16[128,2048]{1,0:T(8,128)(2,1)S(1)} %collective-permute-done.17.refs_2_), channel_id=1, source_target_pairs={{0,4},{4,0},{8,12},{12,8},{16,20},{20,16},{24,28},{28,24},{1,5},{5... | collective-permute-start | bytes 1572872 | tf_op jit(solution)/shard_map/ppermute | solution.py:393
  78.2 28.1 %collective-permute-start.30 = (bf16[128,2048]{1,0:T(8,128)(2,1)S(1)}, bf16[128,2048]{1,0:T(8,128)(2,1)S(1)}, u32[]{:S(2)}, u32[]{:S(2)}) collective-permute-start(bf16[128,2048]{1,0:T(8,128)(2,1)S(1)} %collective-permute-done.21.refs_3_), channel_id=1, source_target_pairs={{0,4},{4,0},{8,12},{12,8},{16,20},{20,16},{24,28},{28,24},{1,5},{5... | collective-permute-start | bytes 1572872 | tf_op jit(solution)/shard_map/ppermute | solution.py:393
  83.8 23.0 %collective-permute-start.22 = (bf16[128,2048]{1,0:T(8,128)(2,1)S(1)}, bf16[128,2048]{1,0:T(8,128)(2,1)S(1)}, u32[]{:S(2)}, u32[]{:S(2)}) collective-permute-start(bf16[128,2048]{1,0:T(8,128)(2,1)S(1)} %collective-permute-done.21.refs_3_), channel_id=1, source_target_pairs={{0,8},{4,12},{8,16},{12,20},{16,24},{20,28},{24,0},{28,4},{1,9},{5... | collective-permute-start | bytes 1572872 | tf_op jit(solution)/shard_map/ppermute | solution.py:388
  89.7 25.8 %collective-permute-start.7 = (bf16[2,512,256]{2,1,0:T(8,128)(2,1)S(1)}, bf16[2,512,256]{2,1,0:T(8,128)(2,1)S(1)}, u32[]{:S(2)}, u32[]{:S(2)}) collective-permute-start(bf16[2,512,256]{2,1,0:T(8,128)(2,1)S(1)} %pad_maximum_fusion.1.refs_0_), channel_id=1, source_target_pairs={{0,1},{1,0},{2,3},{3,2},{4,5},{5,4},{6,7},{7,6},{8,9},{9,8},{10,11... | collective-permute-start | bytes 1572872 | tf_op jit(solution)/shard_map/ppermute | solution.py:456
  89.8 28.8 %collective-permute-start.40 = (bf16[2,512,256]{2,1,0:T(8,128)(2,1)S(1)}, bf16[2,512,256]{2,1,0:T(8,128)(2,1)S(1)}, u32[]{:S(2)}, u32[]{:S(2)}) collective-permute-start(bf16[2,512,256]{2,1,0:T(8,128)(2,1)S(1)} %pad_maximum_fusion.1.refs_0_), channel_id=1, source_target_pairs={{0,4},{4,0},{8,12},{12,8},{16,20},{20,16},{24,28},{28,24},{1,5},{5... | collective-permute-start | bytes 1572872 | tf_op jit(solution)/shard_map/ppermute | solution.py:448
  95.0 24.9 %collective-permute-start.18 = (bf16[128,2048]{1,0:T(8,128)(2,1)S(1)}, bf16[128,2048]{1,0:T(8,128)(2,1)S(1)}, u32[]{:S(2)}, u32[]{:S(2)}) collective-permute-start(bf16[128,2048]{1,0:T(8,128)(2,1)S(1)} %collective-permute-done.17.refs_2_), channel_id=1, source_target_pairs={{0,8},{4,12},{8,16},{12,20},{16,24},{20,28},{24,0},{28,4},{1,9},{5... | collective-permute-start | bytes 1572872 | tf_op jit(solution)/shard_map/ppermute | solution.py:388
  119.9 19.7 %collective-permute-start.19 = (bf16[128,2048]{1,0:T(8,128)(2,1)S(1)}, bf16[128,2048]{1,0:T(8,128)(2,1)S(1)}, u32[]{:S(2)}, u32[]{:S(2)}) collective-permute-start(bf16[128,2048]{1,0:T(8,128)(2,1)S(1)} %collective-permute-done.18.refs_0_), channel_id=1, source_target_pairs={{0,4},{4,0},{8,12},{12,8},{16,20},{20,16},{24,28},{28,24},{1,5},{5... | collective-permute-start | bytes 1572872 | tf_op jit(solution)/shard_map/ppermute | solution.py:393
  127.8 16.7 %collective-permute-start.3 = (bf16[1,512,256]{2,1,0:T(8,128)(2,1)S(1)}, bf16[1,512,256]{2,1,0:T(8,128)(2,1)S(1)}, u32[]{:S(2)}, u32[]{:S(2)}) collective-permute-start(bf16[1,512,256]{2,1,0:T(8,128)(2,1)S(1)} %bitcast.32), channel_id=1, source_target_pairs={{0,4},{4,0},{8,12},{12,8},{16,20},{20,16},{24,28},{28,24},{1,5},{5... | collective-permute-start | bytes 786440 | tf_op jit(solution)/shard_map/ppermute | solution.py:448
  128.6 24.1 %collective-permute-start.9 = (bf16[2,512,256]{2,1,0:T(8,128)(2,1)S(1)}, bf16[2,512,256]{2,1,0:T(8,128)(2,1)S(1)}, u32[]{:S(2)}, u32[]{:S(2)}) collective-permute-start(bf16[2,512,256]{2,1,0:T(8,128)(2,1)S(1)} %collective-permute-done.8.refs_2_), channel_id=1, source_target_pairs={{0,1},{1,0},{2,3},{3,2},{4,5},{5,4},{6,7},{7,6},{8,9},{9,8},{10,11... | collective-permute-start | bytes 1572872 | tf_op jit(solution)/shard_map/ppermute | solution.py:456
  129.9 22.7 %collective-permute-start.42 = (bf16[2,512,256]{2,1,0:T(8,128)(2,1)S(1)}, bf16[2,512,256]{2,1,0:T(8,128)(2,1)S(1)}, u32[]{:S(2)}, u32[]{:S(2)}) collective-permute-start(bf16[2,512,256]{2,1,0:T(8,128)(2,1)S(1)} %collective-permute-done.40.refs_0_), channel_id=1, source_target_pairs={{0,2},{1,3},{2,0},{3,1},{4,6},{5,7},{6,4},{7,5},{8,10},{9,11},{10,... | collective-permute-start | bytes 1572872 | tf_op jit(solution)/shard_map/ppermute | solution.py:452
  152.6 28.1 %collective-permute-start.41 = (bf16[2,512,256]{2,1,0:T(8,128)(2,1)S(1)}, bf16[2,512,256]{2,1,0:T(8,128)(2,1)S(1)}, u32[]{:S(2)}, u32[]{:S(2)}) collective-permute-start(bf16[2,512,256]{2,1,0:T(8,128)(2,1)S(1)} %collective-permute-done.40.refs_0_), channel_id=1, source_target_pairs={{0,1},{1,0},{2,3},{3,2},{4,5},{5,4},{6,7},{7,6},{8,9},{9,8},{10,11... | collective-permute-start | bytes 1572872 | tf_op jit(solution)/shard_map/ppermute | solution.py:456
  152.6 28.1 %collective-permute-start.43 = (bf16[2,512,256]{2,1,0:T(8,128)(2,1)S(1)}, bf16[2,512,256]{2,1,0:T(8,128)(2,1)S(1)}, u32[]{:S(2)}, u32[]{:S(2)}) collective-permute-start(bf16[2,512,256]{2,1,0:T(8,128)(2,1)S(1)} %collective-permute-done.42.refs_2_), channel_id=1, source_target_pairs={{0,1},{1,0},{2,3},{3,2},{4,5},{5,4},{6,7},{7,6},{8,9},{9,8},{10,11... | collective-permute-start | bytes 1572872 | tf_op jit(solution)/shard_map/ppermute | solution.py:456
  158.0 17.8 %collective-permute-start.36 = (bf16[256,256]{1,0:T(8,128)(2,1)S(1)}, bf16[256,256]{1,0:T(8,128)(2,1)S(1)}, u32[]{:S(2)}, u32[]{:S(2)}) collective-permute-start(bf16[256,256]{1,0:T(8,128)(2,1)S(1)} %get-tuple-element.76), channel_id=1, source_target_pairs={{0,16},{4,20},{8,24},{12,28},{16,0},{20,4},{24,8},{28,12},{1,17},{... | collective-permute-start | bytes 393224 | tf_op jit(solution)/shard_map/ppermute | solution.py:435
  159.8 17.8 %collective-permute-start.37 = (bf16[256,256]{1,0:T(8,128)(2,1)S(1)}, bf16[256,256]{1,0:T(8,128)(2,1)S(1)}, u32[]{:S(2)}, u32[]{:S(2)}) collective-permute-start(bf16[256,256]{1,0:T(8,128)(2,1)S(1)} %get-tuple-element.77), channel_id=1, source_target_pairs={{0,20},{4,16},{8,28},{12,24},{16,4},{20,0},{24,12},{28,8},{1,21},{... | collective-permute-start | bytes 393224 | tf_op jit(solution)/shard_map/ppermute | solution.py:435
  (27 other events, 273.4 us)
